TPU v7x, 32 devices: a whole 2x2x4 slice. The times are simulated.
32 devices in a mesh: rep: 2 (over x), fs: 8 (over z, y), tp: 2 (over core).
Axes of the slice: x: 2, y: 2, z: 4, core: 2. Of those that a mesh axis runs over, the one named last changes fastest.
Arguments:
- x_early: bfloat16 [1792, 2048], P(('rep', 'fs')), may hold values from -6 to 6
- x_late: bfloat16 [1792, 2048], P(('rep', 'fs')), may hold values from -6 to 6
- grad_out: bfloat16 [1792, 2048], P(('rep', 'fs')), may hold values from -6 to 6
- w_gate: bfloat16 [2048, 3072], P('fs', 'tp'), may hold values from -0.125 to 0.125
- w_up: bfloat16 [2048, 3072], P('fs', 'tp'), may hold values from -0.125 to 0.125
- w_down: bfloat16 [3072, 2048], P('tp', 'fs'), may hold values from -0.109375 to 0.109375
- gate_sum: float32 [2048, 3072], P('fs', 'tp'), may hold values from -80 to 80
- up_sum: float32 [2048, 3072], P('fs', 'tp'), may hold values from -80 to 80
- down_sum: float32 [3072, 2048], P('tp', 'fs'), may hold values from -80 to 80
Outputs:
- out_late: bfloat16 [1792, 2048], P(('rep', 'fs'))
- grad_in: bfloat16 [1792, 2048], P(('rep', 'fs'))
- new_gate_sum: float32 [2048, 3072], P('fs', 'tp')
- new_up_sum: float32 [2048, 3072], P('fs', 'tp')
- new_down_sum: float32 [3072, 2048], P('tp', 'fs')
All inputs are finite; a program needn't handle non-finite values.
Results may differ from a plain program's by a relative error of at most 0.018.
Values may be sent and summed in bfloat16 or wider, within the bound.
A program may use at most 128 MiB of HBM per device.

v0:
```python
import functools

import jax
import jax.numpy as jnp
from jax import lax
from jax.experimental import pallas as pl
from jax.experimental.pallas import tpu as pltpu
from jax.sharding import PartitionSpec as P

epsilon = 1e-06
MESH = pl.DeviceIdType.MESH
ANY = pl.BlockSpec(memory_space=pl.ANY)
LANES, ROWS = 128, 16


def contract_rows(left, right):
    return lax.dot_general(
        left, right, (((0,), (0,)), ((), ())), preferred_element_type=jnp.float32
    )


def contract_cols(left, right):
    return lax.dot_general(
        left, right, (((1,), (1,)), ((), ())), preferred_element_type=jnp.float32
    )


def greet(peers):
    barrier = pltpu.get_barrier_semaphore()
    for peer in peers:
        pl.semaphore_signal(barrier, inc=1, device_id=peer, device_id_type=MESH)
    pl.semaphore_wait(barrier, len(peers))


def push(src, dst, send_sem, recv_sem, peer):
    copy = pltpu.make_async_remote_copy(
        src_ref=src,
        dst_ref=dst,
        send_sem=send_sem,
        recv_sem=recv_sem,
        device_id=peer,
        device_id_type=MESH,
    )
    return copy


def block(index, size, unit):
    return pl.ds(pl.multiple_of(index * size, unit), size)


def call(body, outs, sems, collective, *args, scratch=()):
    return pl.pallas_call(
        body,
        out_shape=outs,
        in_specs=[ANY] * len(args),
        out_specs=jax.tree.map(lambda _: ANY, outs),
        scratch_shapes=[pltpu.SemaphoreType.DMA((n,)) for n in sems] + list(scratch),
        compiler_params=pltpu.CompilerParams(
            collective_id=collective, has_side_effects=True, vmem_limit_bytes=2**20
        ),
    )(*args)


def here():
    rep, fs, tp = lax.axis_index("rep"), lax.axis_index("fs"), lax.axis_index("tp")
    return rep, fs, tp, {"rep": 1 - rep}, {"tp": 1 - tp}


def gather_kernel(n, acts, weights, acts_all, weights_all, send, recv, wsend, wrecv):
    rep, fs, tp, twin, mate = here()
    line = n // 2
    z, y = fs // 2, lax.rem(fs, 2)
    side = {"fs": fs + 1 - 2 * y}
    rows, width = acts.shape[1], acts.shape[2]
    half = width // 2
    piece = weights_all.shape[1]
    part = piece // 2
    depth = weights.shape[2]
    mine = block(tp, half, LANES)
    greet([twin, mate] + [{"fs": lax.rem(fs + k, n)} for k in range(1, n)])

    def spot(origin):
        return acts_all.at[:, block(origin, rows, ROWS), mine]

    def other_spot(origin):
        return acts_all.at[:, block(origin, rows, ROWS), block(1 - tp, half, LANES)]

    right0, left0, side0, mate0 = 1, 1 + line, 1 + 2 * line, 1 + 3 * line
    own = acts.at[:, :, mine]
    up, down = {"fs": lax.rem(fs + 2, n)}, {"fs": lax.rem(fs + n - 2, n)}

    def go_up(s):
        src = own if s == 0 else spot(fs - 2 * s)
        return push(src, spot(fs - 2 * s), send.at[right0 + s], recv.at[right0 + s], up)

    def go_down(s):
        src = own if s == 0 else spot(fs + 2 * s)
        return push(src, spot(fs + 2 * s), send.at[left0 + s], recv.at[left0 + s], down)

    def go_side(s, sign):
        origin = fs + 2 * sign * s
        src = own if s == 0 else spot(origin)
        at = side0 + origin // 2
        return push(src, spot(origin), send.at[at], recv.at[at], side)

    def go_mate(origin):
        at = mate0 + origin
        return push(spot(origin), spot(origin), send.at[at], recv.at[at], mate)

    def weight(k):
        to = lax.rem(fs + k, n)
        src = weights.at[:, block(to * 2 + rep, part, ROWS), :]
        dst = weights_all.at[:, block(rep, part, ROWS), block(fs, depth, LANES)]
        return push(src, dst, wsend.at[k], wrecv.at[k], {"fs": to})

    def weight_on(k):
        origin = lax.rem(fs + n - k, n)
        ref = weights_all.at[:, block(rep, part, ROWS), block(origin, depth, LANES)]
        return push(ref, ref, wsend.at[n + k], wrecv.at[n + k], twin)

    def weight_from_twin(k):
        origin = lax.rem(fs + n - k, n)
        ref = weights_all.at[:, block(1 - rep, part, ROWS), block(origin, depth, LANES)]
        return push(ref, ref, wsend.at[n + k], wrecv.at[n + k], twin)

    own_weight = push(
        weights.at[:, block(fs, piece, ROWS), :],
        weights_all.at[:, :, block(fs, depth, LANES)],
        wsend.at[0],
        wrecv.at[0],
        twin,
    )
    own_mate = push(acts, acts_all.at[:, block(fs, rows, ROWS), :], send.at[0], recv.at[0], mate)

    has_up = lambda s: (z - s >= 0) & (z + 1 < line)
    has_down = lambda s: (z + s < line) & (z - 1 >= 0)
    from_below = lambda s: z - 1 - s >= 0
    from_above = lambda s: z + 1 + s < line

    pl.when(has_up(0))(lambda: go_up(0).start())
    pl.when(has_down(0))(lambda: go_down(0).start())
    go_side(0, 1).start()
    own_mate.start()
    own_weight.start()
    order = sorted(range(1, n), key=lambda k: -min(k, n - k))
    groups = [order[g :: line] for g in range(line)]

    for s in range(line - 1):
        for k in groups[s]:
            weight(k).start()

        def below():
            push(spot(fs - 2 * (s + 1)), spot(fs - 2 * (s + 1)), send.at[right0 + s], recv.at[right0 + s], up).wait_recv()
            if s + 1 < line - 1:
                pl.when(has_up(s + 1))(lambda: go_up(s + 1).start())
            go_side(s + 1, -1).start()
            go_mate(fs - 2 * (s + 1)).start()

        def above():
            push(spot(fs + 2 * (s + 1)), spot(fs + 2 * (s + 1)), send.at[left0 + s], recv.at[left0 + s], up).wait_recv()
            if s + 1 < line - 1:
                pl.when(has_down(s + 1))(lambda: go_down(s + 1).start())
            go_side(s + 1, 1).start()
            go_mate(fs + 2 * (s + 1)).start()

        pl.when(from_below(s))(below)
        pl.when(from_above(s))(above)
    for k in groups[line - 1]:
        weight(k).start()

    def side_in(place):
        origin = place * 2 + (1 - y)
        at = side0 + place
        push(spot(origin), spot(origin), send.at[at], recv.at[at], side).wait_recv()
        go_mate(origin).start()

    side_in(z)
    for k in order:
        origin = lax.rem(fs + n - k, n)
        ref = weights_all.at[:, block(rep, part, ROWS), block(origin, depth, LANES)]
        push(ref, ref, wsend.at[k], wrecv.at[k], twin).wait_recv()
        weight_on(k).start()
    for s in range(1, line):
        pl.when(z - s >= 0)(lambda: side_in(z - s))
        pl.when(z + s < line)(lambda: side_in(z + s))

    own_mate.wait()
    own_weight.wait()
    for k in range(1, n):
        weight_from_twin(k).wait_recv()
        weight_on(k).wait_send()
        weight(k).wait_send()
        origin = lax.rem(fs + k, n)
        at = mate0 + origin
        ref = other_spot(origin)
        push(ref, ref, send.at[at], recv.at[at], mate).wait()
    for s in range(line - 1):
        pl.when(has_up(s))(lambda: go_up(s).wait_send())
        pl.when(has_down(s))(lambda: go_down(s).wait_send())
    for place in range(line):
        ref = spot(place * 2 + y)
        push(ref, ref, send.at[side0 + place], recv.at[side0 + place], side).wait_send()


def add_rows(dst, left, right):
    strip = ROWS
    count = dst.shape[0] // strip

    @pl.loop(0, count)
    def _(i):
        at = pl.ds(pl.multiple_of(i * strip, strip), strip)
        total = left[at, :].astype(jnp.float32) + right[at, :].astype(jnp.float32)
        dst[at, :] = total.astype(dst.dtype)


def reduce_kernel(
    n,
    late,
    norm,
    gate_up,
    down,
    full,
    grads_all,
    p_in,
    p2,
    y_in,
    p3,
    z_in,
    g_in,
    g2,
    sums,
    send,
    recv,
    gsend,
    grecv,
    local,
):
    rep, fs, tp, twin, mate = here()
    line = n // 2
    z, y = fs // 2, lax.rem(fs, 2)
    side = {"fs": fs + 1 - 2 * y}
    half = sums.shape[2]
    rows = sums.shape[1]
    part = g2.shape[1]
    piece = 2 * part
    depth = grads_all.shape[2]
    mine, other = block(tp, half, LANES), block(1 - tp, half, LANES)
    greet([twin, mate] + [{"fs": lax.rem(fs + k, n)} for k in range(1, n)])
    order = sorted(range(1, line), key=lambda k: -min(k, line - k)) + [0]
    far = sorted(range(1, n), key=lambda k: -min(k, n - k))
    side0, line0, x0, last = 2 * line, 3 * line, 4 * line, 4 * line + 3

    def place(k):
        return lax.rem(z + k, line)

    def span(k):
        return block(place(k), 2 * rows, ROWS)

    def to_mate(i, k):
        src = (late, norm)[i].at[span(k), other]
        at = i * line + k
        return push(src, p_in.at[i, span(k), :], send.at[at], recv.at[at], mate)

    def to_side(k):
        src = p2.at[:, block(place(k) * 2 + 1 - y, rows, ROWS), :]
        at = side0 + k
        return push(src, y_in.at[:, place(k)], send.at[at], recv.at[at], side)

    def to_line(k):
        at = line0 + k
        return push(
            p3.at[k], z_in.at[k - 1], send.at[at], recv.at[at], {"fs": lax.rem(fs + 2 * k, n)}
        )

    def delta(a, who):
        if a < 2:
            return gate_up.at[block(2 * a + who, part, ROWS), :]
        return down.at[block(who, part, ROWS), :]

    def to_twin(a):
        return push(delta(a, 1 - rep), g_in.at[a], send.at[x0 + a], recv.at[x0 + a], twin)

    def slot(a, origin, who):
        return grads_all.at[a, block(origin * 2 + who, part, ROWS), :]

    def share(a, k):
        to = lax.rem(fs + k, n)
        src = g2.at[a, :, block(to, depth, LANES)]
        at = a * n + k
        return push(src, slot(a, fs, rep), gsend.at[at], grecv.at[at], {"fs": to})

    def share_in(a, k):
        ref = slot(a, lax.rem(fs + n - k, n), rep)
        at = a * n + k
        return push(ref, ref, gsend.at[at], grecv.at[at], twin)

    def share_on(a, k):
        ref = slot(a, lax.rem(fs + n - k, n), rep)
        at = (3 + a) * n + k
        return push(ref, ref, gsend.at[at], grecv.at[at], twin)

    def share_from_twin(a, k):
        ref = slot(a, lax.rem(fs + n - k, n), 1 - rep)
        at = (3 + a) * n + k
        return push(ref, ref, gsend.at[at], grecv.at[at], twin)

    def own(a):
        return g2.at[a, :, block(fs, depth, LANES)]

    def own_twin(a):
        at = (3 + a) * n
        return push(own(a), slot(a, fs, rep), gsend.at[at], grecv.at[at], twin)

    def own_put(a):
        return pltpu.make_async_copy(own(a), slot(a, fs, rep), local.at[a])

    def weight_step(a):
        to_twin(a).wait_recv()
        add_rows(g2.at[a], delta(a, rep), g_in.at[a])
        for k in far:
            share(a, k).start()
        own_twin(a).start()
        own_put(a).start()

    def forward(a):
        for k in far:
            share_in(a, k).wait_recv()
            share_on(a, k).start()

    for k in order:
        for i in range(2):
            to_mate(i, k).start()
    for a in range(3):
        to_twin(a).start()
    for k in order:
        for i in range(2):
            to_mate(i, k).wait_recv()
            src = (late, norm)[i].at[span(k), mine]
            add_rows(p2.at[i, span(k), :], src, p_in.at[i, span(k), :])
        to_side(k).start()
    weight_step(0)
    for step, k in enumerate(order):
        to_side(k).wait_recv()
        for i in range(2):
            src = p2.at[i, block(place(k) * 2 + y, rows, ROWS), :]
            add_rows(p3.at[k, i], src, y_in.at[i, place(k)])
        if k:
            to_line(k).start()
        if step < 2:
            weight_step(step + 1)
        if step >= 1:
            if step - 1 < 3:
                forward(step - 1)
    for a in range(max(len(order) - 1, 0), 3):
        forward(a)
    for k in order[:-1]:
        to_line(k).wait_recv()
    for i in range(2):

        @pl.loop(0, rows // ROWS)
        def _(j):
            at = pl.ds(pl.multiple_of(j * ROWS, ROWS), ROWS)
            total = p3[0, i, at, :].astype(jnp.float32)
            for k in range(1, line):
                total += z_in[k - 1, i, at, :].astype(jnp.float32)
            sums[i, at, :] = total.astype(sums.dtype)

    out = push(sums, full.at[:, :, mine], send.at[last], recv.at[last], mate)
    out.start()
    keep = pltpu.make_async_copy(sums, full.at[:, :, mine], local.at[3])
    keep.start()
    for a in range(3):
        own_put(a).wait()
        own_twin(a).wait_send()
        ref = slot(a, fs, 1 - rep)
        at = (3 + a) * n
        push(ref, ref, gsend.at[at], grecv.at[at], twin).wait_recv()
        to_twin(a).wait_send()
        for k in far:
            share(a, k).wait_send()
            share_on(a, k).wait_send()
            share_from_twin(a, k).wait_recv()
    for k in order:
        for i in range(2):
            to_mate(i, k).wait_send()
        to_side(k).wait_send()
        if k:
            to_line(k).wait_send()
    keep.wait()
    out.wait_send()
    push(sums, full.at[:, :, other], send.at[last], recv.at[last], mate).wait_recv()


def update_kernel(gate_sum, up_sum, down_sum, deltas, new_gate, new_up, new_down):
    new_gate[...] = gate_sum[...] + deltas[0].astype(jnp.float32).T
    new_up[...] = up_sum[...] + deltas[1].astype(jnp.float32).T
    new_down[...] = down_sum[...] + deltas[2].astype(jnp.float32)


def update(gate_sum, up_sum, down_sum, deltas):
    depth, hidden_here = gate_sum.shape
    step = next(b for b in (512, 256, 128) if hidden_here % b == 0)
    wide = pl.BlockSpec((depth, step), lambda i: (0, i))
    tall = pl.BlockSpec((step, depth), lambda i: (i, 0))
    size = depth * hidden_here
    return pl.pallas_call(
        update_kernel,
        grid=(hidden_here // step,),
        out_shape=[jax.ShapeDtypeStruct(v.shape, v.dtype) for v in (gate_sum, up_sum, down_sum)],
        in_specs=[wide, wide, tall, pl.BlockSpec((3, step, depth), lambda i: (0, i, 0))],
        out_specs=[wide, wide, tall],
        cost_estimate=pl.CostEstimate(flops=3 * size, bytes_accessed=30 * size, transcendentals=0),
    )(gate_sum, up_sum, down_sum, deltas)


def fast_shards(n, x_early, x_late, grad_out, w_gate, w_up, w_down, gate_sum, up_sum, down_sum):
    bf16, f32 = jnp.bfloat16, jnp.float32
    shape = jax.ShapeDtypeStruct
    rep, fs, tp = lax.axis_index("rep"), lax.axis_index("fs"), lax.axis_index("tp")
    line = n // 2
    y = lax.rem(fs, 2)
    rows, width = x_early.shape
    hidden_here, depth = w_down.shape
    piece = hidden_here // n
    half = width // 2
    early = x_early.astype(f32)
    late = x_late.astype(f32)
    scale_of = lambda v: lax.rsqrt(jnp.mean(v * v, axis=-1, keepdims=True) + epsilon)
    early_scale, late_scale = scale_of(early), scale_of(late)
    acts = jnp.stack(
        [(early * early_scale).astype(bf16), (late * late_scale).astype(bf16), grad_out]
    )
    weights = jnp.stack([w_gate.T, w_up.T, w_down])
    acts_all, weights_all = call(
        functools.partial(gather_kernel, n),
        [shape((3, n * rows, width), bf16), shape((3, piece, width), bf16)],
        (1 + 3 * line + n, 1 + 3 * line + n, 2 * n, 2 * n),
        0,
        acts,
        weights,
    )
    gate_t, up_t, down_t = weights_all[0], weights_all[1], weights_all[2]
    normed, cotangent = acts_all[0], acts_all[2]
    gate_up = weights_all[:2].reshape(2 * piece, width)
    def activations(rows_in):
        pre = contract_cols(rows_in, gate_up)
        gate_pre, up_pre = pre[:, :piece], pre[:, piece:]
        sig = jax.nn.sigmoid(gate_pre)
        return gate_pre, up_pre, sig, (gate_pre * sig * up_pre).astype(bf16)

    tokens = n * rows
    g, u, s, hidden = activations(normed)
    hidden_late = activations(acts_all[1])[3]
    late_part = jnp.dot(hidden_late, down_t, preferred_element_type=f32).astype(bf16)
    grad_hidden = 0.5 * contract_cols(cotangent, down_t)
    grad_gate_in = (grad_hidden * u * s * (1.0 + g * (1.0 - s))).astype(bf16)
    grad_up_in = (grad_hidden * g * s).astype(bf16)
    grads_in = jnp.concatenate([grad_gate_in, grad_up_in], axis=1)
    normed_part = jnp.dot(grads_in, gate_up, preferred_element_type=f32).astype(bf16)
    gate_up_delta = contract_rows(grads_in, normed).astype(bf16)
    down_delta = (0.5 * contract_rows(hidden, cotangent)).astype(bf16)
    part = piece // 2
    dma = pltpu.SemaphoreType.DMA
    vmem = pl.BlockSpec(memory_space=pltpu.VMEM)
    full, grads_all = pl.pallas_call(
        functools.partial(reduce_kernel, n),
        out_shape=[shape((2, rows, width), bf16), shape((3, hidden_here, depth), bf16)],
        in_specs=[vmem] * 4,
        out_specs=[ANY, ANY],
        scratch_shapes=[
            pltpu.VMEM((2, tokens, half), bf16),
            pltpu.VMEM((2, tokens, half), bf16),
            pltpu.VMEM((2, line, rows, half), bf16),
            pltpu.VMEM((line, 2, rows, half), bf16),
            pltpu.VMEM((line - 1, 2, rows, half), bf16),
            pltpu.VMEM((3, part, width), bf16),
            pltpu.VMEM((3, part, width), bf16),
            pltpu.VMEM((2, rows, half), bf16),
            dma((4 * line + 4,)),
            dma((4 * line + 4,)),
            dma((6 * n,)),
            dma((6 * n,)),
            dma((4,)),
        ],
        compiler_params=pltpu.CompilerParams(
            collective_id=1, has_side_effects=True, vmem_limit_bytes=48 * 2**20
        ),
    )(late_part, normed_part, gate_up_delta, down_delta)
    full = full.astype(f32)
    branch, grad_normed = full[0], full[1]
    out_late = (late + 0.5 * branch).astype(bf16)
    unit_rows = early * early_scale
    inner = jnp.mean(grad_normed * unit_rows, axis=-1, keepdims=True)
    grad_in = (
        grad_out.astype(f32) + early_scale * (grad_normed - unit_rows * inner)
    ).astype(bf16)
    return (out_late, grad_in, *update(gate_sum, up_sum, down_sum, grads_all))


def shards(x_early, x_late, grad_out, w_gate, w_up, w_down, gate_sum, up_sum, down_sum):
    gate_full, up_full, down_full = (
        lax.all_gather(w_gate, "fs", axis=0, tiled=True),
        lax.all_gather(w_up, "fs", axis=0, tiled=True),
        lax.all_gather(w_down, "fs", axis=1, tiled=True),
    )
    batch_rows = x_early.shape[0]
    stacked = jnp.concatenate([x_early, x_late], axis=0).astype(jnp.float32)
    row_scale = lax.rsqrt(jnp.mean(stacked * stacked, axis=-1, keepdims=True) + epsilon)
    normed = (stacked * row_scale).astype(jnp.bfloat16)
    gate_pre = jnp.dot(normed, gate_full, preferred_element_type=jnp.float32)
    up_pre = jnp.dot(normed, up_full, preferred_element_type=jnp.float32)
    gate_sig = jax.nn.sigmoid(gate_pre)
    hidden = (gate_pre * gate_sig * up_pre).astype(jnp.bfloat16)
    late_part = jnp.dot(hidden[batch_rows:], down_full, preferred_element_type=jnp.float32).astype(
        jnp.bfloat16
    )
    branch = lax.psum(late_part, "tp").astype(jnp.float32)
    out_late = (stacked[batch_rows:] + 0.5 * branch).astype(jnp.bfloat16)
    early_gate = gate_pre[:batch_rows]
    early_upper = up_pre[:batch_rows]
    early_sig = gate_sig[:batch_rows]
    early_hidden = hidden[:batch_rows]
    early_normed = normed[:batch_rows]
    early_scale = row_scale[:batch_rows]
    grad_hidden = 0.5 * contract_cols(grad_out, down_full)
    grad_gate_in = (
        grad_hidden * early_upper * early_sig * (1.0 + early_gate * (1.0 - early_sig))
    ).astype(jnp.bfloat16)
    grad_up_in = (grad_hidden * early_gate * early_sig).astype(jnp.bfloat16)
    normed_part = contract_cols(grad_gate_in, gate_full) + contract_cols(grad_up_in, up_full)
    grad_normed = lax.psum(normed_part.astype(jnp.bfloat16), "tp").astype(jnp.float32)
    unit_rows = stacked[:batch_rows] * early_scale
    inner = jnp.mean(grad_normed * unit_rows, axis=-1, keepdims=True)
    grad_in = (
        grad_out.astype(jnp.float32) + early_scale * (grad_normed - unit_rows * inner)
    ).astype(jnp.bfloat16)
    normed_cols, out_cols = (
        lax.all_to_all(early_normed, "fs", split_axis=1, concat_axis=0, tiled=True),
        lax.all_to_all(grad_out, "fs", split_axis=1, concat_axis=0, tiled=True),
    )
    gate_delta = contract_rows(normed_cols, lax.all_gather(grad_gate_in, "fs", axis=0, tiled=True))
    up_delta = contract_rows(normed_cols, lax.all_gather(grad_up_in, "fs", axis=0, tiled=True))
    down_half = contract_rows(lax.all_gather(early_hidden, "fs", axis=0, tiled=True), out_cols)
    down_delta = 0.5 * down_half
    gate_delta, up_delta, down_delta = (
        lax.psum(gate_delta.astype(jnp.bfloat16), "rep").astype(jnp.float32),
        lax.psum(up_delta.astype(jnp.bfloat16), "rep").astype(jnp.float32),
        lax.psum(down_delta.astype(jnp.bfloat16), "rep").astype(jnp.float32),
    )
    return (out_late, grad_in, gate_sum + gate_delta, up_sum + up_delta, down_sum + down_delta)


def shards_for(mesh):
    n, reps, cores = mesh.shape["fs"], mesh.shape["rep"], mesh.shape["tp"]

    def run(*args):
        rows, width = args[0].shape
        hidden_here, depth = args[5].shape
        fits = (
            reps == 2
            and cores == 2
            and n % 2 == 0
            and rows % ROWS == 0
            and width % (2 * LANES) == 0
            and depth % LANES == 0
            and hidden_here % (2 * n * ROWS) == 0
            and hidden_here % LANES == 0
        )
        return fast_shards(n, *args) if fits else shards(*args)

    return run


def solution(mesh):
    placed = (
        P(("rep", "fs"), None),
        P(("rep", "fs"), None),
        P(("rep", "fs"), None),
        P("fs", "tp"),
        P("fs", "tp"),
        P("tp", "fs"),
        P("fs", "tp"),
        P("fs", "tp"),
        P("tp", "fs"),
    )
    return jax.shard_map(
        shards_for(mesh),
        mesh=mesh,
        in_specs=placed,
        out_specs=(
            P(("rep", "fs"), None),
            P(("rep", "fs"), None),
            P("fs", "tp"),
            P("fs", "tp"),
            P("tp", "fs"),
        ),
        check_vma=False,
    )
```

profile of v0, /device:TPU:0, one launch (start us, length us, event | category | flops | bytes accessed | tf_op | source)
XLA Modules:
  0.0 207.5 jit_solution(4451161959627802324)
XLA Ops:
  0.6 1.3 fusion.36
  1.9 1.3 fusion.35
  3.2 1.4 copy.14
  4.7 0.3 copy.15
  5.0 0.3 pad_maximum_fusion.weights
  5.2 0.7 copy-done.1
  6.0 0.1 copy-done.2
  6.1 0.2 fusion.45
  6.3 0.8 copy-done.3
  7.1 0.2 pad_maximum_fusion.1.acts
  7.3 95.8 %shard_map.128 = (bf16[3,896,2048]{2,1,0:T(8,128)(2,1)S(1)}, bf16[3,192,2048]{2,1,0:T(8,128)(2,1)S(1)}) custom-call(bf16[3,112,2048]{2,1,0:T(8,128)(2,1)S(1)} %pad_maximum_fusion.1.acts, bf16[3,1536,256]{2,1,0:T(8,128)(2,1)S(1)} %pad_maximum_fusion.weights), custom_call_target="tpu_custom_call" | custom-call | tf_op jit(solution)/shard_map/pallas_call | solution.py:52
  103.2 1.8 fusion.2
  105.0 1.5 multiply_convert_fusion.2
  106.5 1.0 fusion.21.down
  107.6 1.8 fusion.8
  109.4 1.8 fusion.15.gate_up
  111.2 3.0 %convolution_convert_fusion.1.late = bf16[896,2048]{1,0:T(8,128)(2,1)} fusion(bf16[3,192,2048]{2,1,0:T(8,128)(2,1)S(1)} %get-tuple-element.13, f32[896,384]{0,1:T(8,128)S(1)} %fusion.8), kind=kOutput, calls=%fused_computation.12 | convolution fusion | flops 707510272 | bytes 5832704 | tf_op jit(solution)/shard_map/dot_general | solution.py:454
  114.2 3.9 %convolution_convert_fusion.norm = bf16[896,2048]{1,0:T(8,128)(2,1)} fusion(bf16[384,2048]{1,0:T(8,128)(2,1)S(1)} %bitcast.61, bf16[896,192]{0,1:T(8,128)(2,1)S(1)} %get-tuple-element.20, bf16[896,192]{0,1:T(8,128)(2,1)S(1)} %get-tuple-element.19), kind=kOutput, calls=%fused_computation.11 | convolution fusion | flops 1412497408 | bytes 5931008 | tf_op jit(solution)/shard_map/dot_general | solution.py:459
  118.1 80.7 %shard_map.129 = (bf16[2,112,2048]{2,1,0:T(8,128)(2,1)S(1)}, bf16[3,1536,256]{2,1,0:T(8,128)(2,1)S(1)}) custom-call(bf16[896,2048]{1,0:T(8,128)(2,1)} %convolution_convert_fusion.1.late, bf16[896,2048]{1,0:T(8,128)(2,1)} %convolution_convert_fusion.norm, bf16[384,2048]{1,0:T(8,128)(2,1)S(1)} %fusion.15.gate_up, bf16[192,2048]{1,0:T(8,128)(2,1)S(1)} %fusion.21.down), custom_call_target="tpu_custom_call" | custom-call | tf_op jit(solution)/shard_map/pallas_call | solution.py:465
  198.8 0.2 convert_element_type.60
  199.0 0.3 fusion.30
  199.3 0.9 copy-done
  200.2 1.4 fusion.34
  201.6 5.9 %shard_map.130 = (f32[256,1536]{1,0:T(8,128)}, f32[256,1536]{1,0:T(8,128)}, f32[1536,256]{1,0:T(8,128)}) custom-call(f32[256,1536]{1,0:T(8,128)} %gate_sum.1, f32[256,1536]{1,0:T(8,128)} %up_sum.1, f32[1536,256]{1,0:T(8,128)} %down_sum.1, bf16[3,1536,256]{2,1,0:T(8,128)(2,1)} %copy-done), custom_call_target="tpu_custom_call" | custom-call | flops 1179648 | bytes 11796480 | tf_op jit(solution)/shard_map/pallas_call | solution.py:406
  (12 shorter events, 0.1 us)
Async XLA Ops:
  0.6 4.0 %copy-start.5 = (bf16[256,1536]{1,0:T(8,128)(2,1)S(1)}, bf16[256,1536]{1,0:T(8,128)(2,1)}, u32[]{:S(2)}) copy-start(bf16[256,1536]{1,0:T(8,128)(2,1)} %param.13) | copy-start | bytes 2359300
  1.9 3.0 %copy-start.4 = (bf16[1536,256]{1,0:T(8,128)(2,1)S(1)}, bf16[1536,256]{1,0:T(8,128)(2,1)}, u32[]{:S(2)}) copy-start(bf16[1536,256]{1,0:T(8,128)(2,1)} %param.14) | copy-start | bytes 2359300
  5.0 1.0 copy-start.1
  5.0 1.1 copy-start.2
  6.1 1.0 copy-start.3
  198.8 1.4 copy-start
where the time goes:
time: 211 us; the launch traced here: 207 us
  Pallas kernels  182 us (86%)
  matrix products  14.9 us (7%)
  other arithmetic  5.04 us (2%)
  local copies, waits for them, and re-layouts  4.4 us (2%)
    pallas_call x1, Pallas kernels, call(): pl.pallas_call(body, out_shape=outs, in_specs=[ANY] * len(args), out_spec...  95.8 us
    pallas_call x1, Pallas kernels, fast_shards(): pl.pallas_call(functools.partial(reduce_kernel, n), out_shape=[shape((2,...  80.7 us
    pallas_call x1, Pallas kernels, update(): pl.pallas_call(update_kernel, grid=(hidden_here // step,), out_shape=[jax...  5.89 us
    dot_general x3, matrix products, contract_cols(): lax.dot_general(left, right, (((1,), (1,)), ((), ())), preferred_element_...  5.13 us
    unnamed x14, local copies, waits for them, and re-layouts  4.3 us

commit v1 on v0

v1 whole, which is shorter than its diff:
```python
import functools

import jax
import jax.numpy as jnp
from jax import lax
from jax.experimental import pallas as pl
from jax.experimental.pallas import tpu as pltpu
from jax.sharding import PartitionSpec as P

epsilon = 1e-06
MESH = pl.DeviceIdType.MESH
ANY = pl.BlockSpec(memory_space=pl.ANY)
LANES, ROWS = 128, 16


def contract_rows(left, right):
    return lax.dot_general(
        left, right, (((0,), (0,)), ((), ())), preferred_element_type=jnp.float32
    )


def contract_cols(left, right):
    return lax.dot_general(
        left, right, (((1,), (1,)), ((), ())), preferred_element_type=jnp.float32
    )


def greet(peers):
    barrier = pltpu.get_barrier_semaphore()
    for peer in peers:
        pl.semaphore_signal(barrier, inc=1, device_id=peer, device_id_type=MESH)
    pl.semaphore_wait(barrier, len(peers))


def push(src, dst, send_sem, recv_sem, peer):
    copy = pltpu.make_async_remote_copy(
        src_ref=src,
        dst_ref=dst,
        send_sem=send_sem,
        recv_sem=recv_sem,
        device_id=peer,
        device_id_type=MESH,
    )
    return copy


def block(index, size, unit):
    return pl.ds(pl.multiple_of(index * size, unit), size)


def add_strips(dst, left, right):
    @pl.loop(0, dst.shape[0] // ROWS)
    def _(i):
        at = block(i, ROWS, ROWS)
        total = left[at, :].astype(jnp.float32) + right[at, :].astype(jnp.float32)
        dst[at, :] = total.astype(dst.dtype)


def scale_of(v):
    return lax.rsqrt(jnp.mean(v * v, axis=-1, keepdims=True) + epsilon)


def step_kernel(
    n,
    x_early,
    x_late,
    grad_out,
    w_gate,
    w_up,
    w_down,
    out_late,
    grad_in,
    delta_gate,
    delta_up,
    delta_down,
    acts,
    gate_up,
    down,
    hidden,
    grads,
    part,
    part_in,
    sums,
    from_below,
    from_above,
    gate_up_delta,
    down_delta,
    y_gate_up,
    y_down,
    x_gate_up,
    x_down,
    full,
    send,
    recv,
    local,
):
    f32, bf16 = jnp.float32, jnp.bfloat16
    rep, fs, tp = lax.axis_index("rep"), lax.axis_index("fs"), lax.axis_index("tp")
    line = n // 2
    z, y = fs // 2, lax.rem(fs, 2)
    twin, mate, side = {"rep": 1 - rep}, {"tp": 1 - tp}, {"fs": fs + 1 - 2 * y}
    above, below = {"fs": lax.rem(fs + 2, n)}, {"fs": lax.rem(fs + n - 2, n)}
    rows, width = x_early.shape
    layer, depth = down.shape[0], w_gate.shape[0]
    half, deep, tall = width // 2, depth // 2, layer // 2
    mine, other = block(tp, half, LANES), block(1 - tp, half, LANES)
    names, pending = {}, []
    last = line - 1

    def at(*key):
        return names.setdefault(key, len(names))

    def copies(key, srcs, dsts, peer):
        return [
            push(s, d, send.at[at(key, i)], recv.at[at(key, i)], peer)
            for i, (s, d) in enumerate(zip(srcs, dsts))
        ]

    def go(group, cond=None):
        def start():
            for copy in group:
                copy.start()

        pending.append((cond, group))
        if cond is None:
            start()
        else:
            pl.when(cond)(start)

    def arrived(key, refs):
        for copy in copies(key, refs, refs, twin):
            copy.wait_recv()

    def place(k):
        return lax.rem(z + k, line)

    def origin(k):
        return lax.rem(z + line - k, line)

    def slice3(owner, who):
        at_rows = block(owner * 2 + who, deep, ROWS)
        return [
            gate_up.at[at_rows, pl.ds(0, layer)],
            gate_up.at[at_rows, pl.ds(layer, layer)],
            down.at[block(who, tall, ROWS), block(owner, depth, LANES)],
        ]

    def slice2(owner, who):
        return [
            gate_up.at[block(owner * 2 + who, deep, ROWS), :],
            down.at[block(who, tall, ROWS), block(owner, depth, LANES)],
        ]

    def whole3(owner):
        at_rows = block(owner, depth, ROWS)
        return [
            gate_up.at[at_rows, pl.ds(0, layer)],
            gate_up.at[at_rows, pl.ds(layer, layer)],
            down.at[:, block(owner, depth, LANES)],
        ]

    def source3(to):
        at_rows, at_cols = block(rep, deep, ROWS), block(to, layer, LANES)
        return [
            w_gate.at[at_rows, at_cols],
            w_up.at[at_rows, at_cols],
            w_down.at[block(to * 2 + rep, tall, ROWS), :],
        ]

    own_source = [
        w_gate.at[:, block(z, layer, LANES)],
        w_up.at[:, block(z, layer, LANES)],
        w_down.at[block(z, layer, ROWS), :],
    ]
    own_rows = block(z, rows, ROWS)
    keeps = [
        pltpu.make_async_copy(s, d, local.at[i])
        for i, (s, d) in enumerate(zip(own_source, whole3(fs)))
    ]
    keeps.append(pltpu.make_async_copy(grad_out, acts.at[1, own_rows, :], local.at[3]))
    for keep in keeps:
        keep.start()

    barrier = pltpu.get_barrier_semaphore()
    peers = [twin, mate, side] + [{"fs": lax.rem(fs + 2 * k, n)} for k in range(1, line)]
    for peer in peers:
        pl.semaphore_signal(barrier, inc=1, device_id=peer, device_id_type=MESH)
    pl.semaphore_wait(barrier, len(peers))

    for k in sorted(range(1, line), key=lambda k: -min(k, line - k)):
        to = {"fs": lax.rem(fs + 2 * k, n)}
        go(copies(("wz", k), source3(place(k)), slice3(fs, rep), to))
    go(copies("wy0", own_source, whole3(fs), side))

    def normalise(i, x):
        @pl.loop(0, rows // ROWS)
        def _(j):
            v = x[block(j, ROWS, ROWS), :].astype(f32)
            to = pl.ds(pl.multiple_of(z * rows + j * ROWS, ROWS), ROWS)
            acts[i, to, :] = (v * scale_of(v)).astype(bf16)

    def spot(i, place_of, cols=mine):
        return acts.at[i, block(place_of, rows, ROWS), cols]

    def go_up(i, s):
        src = grad_out.at[:, mine] if i == 1 and s == 0 else spot(i, z - s)
        go(copies(("up", i, s), [src], [spot(i, z - s)], above), (z - s >= 0) & (z < last))

    def go_down(i, s):
        src = grad_out.at[:, mine] if i == 1 and s == 0 else spot(i, z + s)
        go(copies(("down", i, s), [src], [spot(i, z + s)], below), (z + s < line) & (z > 0))

    def move(i, s):
        under, over = z - 1 - s, z + 1 + s
        pl.when(under >= 0)(lambda: arrived(("up", i, s), [spot(i, under)]))
        if s + 1 < last:
            go_up(i, s + 1)
        go(copies(("mu", i, s), [spot(i, under)], [spot(i, under)], mate), under >= 0)
        pl.when(over < line)(lambda: arrived(("down", i, s), [spot(i, over)]))
        if s + 1 < last:
            go_down(i, s + 1)
        go(copies(("md", i, s), [spot(i, over)], [spot(i, over)], mate), over < line)

    def moved(i, s):
        under, over = z - 1 - s, z + 1 + s
        pl.when(under >= 0)(lambda: arrived(("mu", i, s), [spot(i, under, other)]))
        pl.when(over < line)(lambda: arrived(("md", i, s), [spot(i, over, other)]))

    def first(i):
        go_up(i, 0)
        go_down(i, 0)

    first(1)
    normalise(0, x_early)
    first(0)
    normalise(2, x_late)

    for k in range(1, line):
        part2 = slice2(origin(k) * 2 + y, rep)
        arrived(("wz", k), slice3(origin(k) * 2 + y, rep))
        go(copies(("wy", k), part2, part2, side))
        go(copies(("wx", k), part2, part2, twin))

    def pass_on(k):
        part2 = slice2(origin(k) * 2 + 1 - y, rep)
        arrived(("wy", k), part2)
        go(copies(("wxx", k), part2, part2, twin))

    for s in range(last - 1):
        move(1, s)
        move(0, s)
        pass_on(s + 1)
    first(2)
    for k in range(max(last, 1), line):
        pass_on(k)
    for keep in keeps:
        keep.wait()
    arrived("wy0", whole3(fs + 1 - 2 * y))
    for k in range(1, line):
        arrived(("wx", k), slice2(origin(k) * 2 + y, 1 - rep))
        arrived(("wxx", k), slice2(origin(k) * 2 + 1 - y, 1 - rep))

    def activations(x):
        pre = jnp.dot(x, gate_up[...], preferred_element_type=f32)
        g, u = pre[:, :layer], pre[:, layer:]
        s = jax.nn.sigmoid(g)
        return g, u, s, (g * s * u).astype(bf16)

    def early_block(place_of):
        here = block(place_of, rows, ROWS)
        g, u, s, h = activations(acts[0, here, :])
        grad_hidden = 0.5 * contract_cols(acts[1, here, :], down[...])
        hidden[here, :] = h
        grads[here, pl.ds(0, layer)] = (grad_hidden * u * s * (1.0 + g * (1.0 - s))).astype(bf16)
        grads[here, pl.ds(layer, layer)] = (grad_hidden * g * s).astype(bf16)

    early_block(z)
    for s in range(last):
        if s == last - 1:
            move(1, s)
            move(0, s)
        moved(1, s)
        moved(0, s)

        @pl.loop(0, 2)
        def _(d):
            to = z + (2 * d - 1) * (s + 1)
            pl.when((to >= 0) & (to < line))(lambda: early_block(to))

    order = list(range(1, line)) + [0]

    def weight_grads(owner):
        cols = block(owner, depth, LANES)
        gate_up_delta[block(owner, depth, ROWS), :] = contract_rows(
            acts[0, :, cols], grads[...]
        ).astype(bf16)
        down_delta[:, cols] = (0.5 * contract_rows(hidden[...], acts[1, :, cols])).astype(bf16)

    def deltas(owner):
        return [
            gate_up_delta.at[block(owner, depth, ROWS), :],
            down_delta.at[:, block(owner, depth, LANES)],
        ]

    for k in order:
        owner = place(k) * 2 + 1 - y
        weight_grads(owner)
        go(copies(("gy", k), deltas(owner), [y_gate_up.at[place(k)], y_down.at[place(k)]], side))

    @pl.loop(0, line)
    def _(t):
        weight_grads(t * 2 + y)

    wide = next(b for b in (512, 256, 128) if width % b == 0)

    @pl.loop(0, width // wide)
    def _(j):
        cols = block(j, wide, LANES)
        part[1, :, cols] = contract_cols(grads[...], gate_up[block(j, wide, ROWS), :]).astype(bf16)

    def to_mate(i):
        go(copies(("pm", i), [part.at[i, :, other]], [part_in.at[i]], mate))

    def from_mate(i):
        arrived(("pm", i), [part_in.at[i]])

        @pl.loop(0, line)
        def _(t):
            here = block(t, rows, ROWS)
            add_strips(sums.at[i, t], part.at[i, here, mine], part_in.at[i, here, :])

    def chain(i):
        for d in range(last):
            t = last - d

            def add_up():
                arrived(("zu", i, t), [from_below.at[i, t]])
                add_strips(sums.at[i, t], sums.at[i, t], from_below.at[i, t])

            pl.when((z >= 1) & (z < t))(add_up)
            go(copies(("zu", i, t), [sums.at[i, t]], [from_below.at[i, t]], above), z < t)

            def add_down():
                arrived(("zd", i, d), [from_above.at[i, d]])
                add_strips(sums.at[i, d], sums.at[i, d], from_above.at[i, d])

            pl.when((z < last) & (z > d))(add_down)
            go(copies(("zd", i, d), [sums.at[i, d]], [from_above.at[i, d]], below), z > d)

    def finish(i):
        for t in range(line):
            if t > 0:

                def add_up():
                    arrived(("zu", i, t), [from_below.at[i, t]])
                    add_strips(sums.at[i, t], sums.at[i, t], from_below.at[i, t])

                pl.when(z == t)(add_up)
            if t < last:

                def add_down():
                    arrived(("zd", i, t), [from_above.at[i, t]])
                    add_strips(sums.at[i, t], sums.at[i, t], from_above.at[i, t])

                pl.when(z == t)(add_down)
        full[i, :, mine] = sums[i, z]
        go(copies(("fm", i), [full.at[i, :, mine]], [full.at[i, :, mine]], mate))

    def outputs():
        for i in range(2):
            arrived(("fm", i), [full.at[i, :, other]])

        @pl.loop(0, rows // ROWS)
        def _(j):
            here = block(j, ROWS, ROWS)
            late = x_late[here, :].astype(f32)
            out_late[here, :] = (late + 0.5 * full[0, here, :].astype(f32)).astype(bf16)
            early = x_early[here, :].astype(f32)
            scale = scale_of(early)
            unit = early * scale
            grad_normed = full[1, here, :].astype(f32)
            inner = jnp.mean(grad_normed * unit, axis=-1, keepdims=True)
            kept = acts[1, pl.ds(pl.multiple_of(z * rows + j * ROWS, ROWS), ROWS), :].astype(f32)
            grad_in[here, :] = (kept + scale * (grad_normed - unit * inner)).astype(bf16)

    def y_step(k):
        t = place(k)
        arrived(("gy", k), [y_gate_up.at[t], y_down.at[t]])
        own = deltas(t * 2 + y)
        add_strips(y_gate_up.at[t], own[0], y_gate_up.at[t])
        add_strips(y_down.at[t], own[1], y_down.at[t])
        srcs = [
            y_gate_up.at[t, block(1 - rep, deep, ROWS), :],
            y_down.at[t, block(1 - rep, tall, ROWS), :],
        ]
        go(copies(("gx", k), srcs, [x_gate_up.at[t], x_down.at[t]], twin))

    def landing(place_of, who):
        at_rows, at_cols = block(who, deep, ROWS), block(place_of, layer, LANES)
        return [
            delta_gate.at[at_rows, at_cols],
            delta_up.at[at_rows, at_cols],
            delta_down.at[block(place_of * 2 + who, tall, ROWS), :],
        ]

    puts = []

    def x_step(k):
        t = place(k)
        arrived(("gx", k), [x_gate_up.at[t], x_down.at[t]])
        add_strips(x_gate_up.at[t], y_gate_up.at[t, block(rep, deep, ROWS), :], x_gate_up.at[t])
        add_strips(x_down.at[t], y_down.at[t, block(rep, tall, ROWS), :], x_down.at[t])
        srcs = [
            x_gate_up.at[t, :, pl.ds(0, layer)],
            x_gate_up.at[t, :, pl.ds(layer, layer)],
            x_down.at[t],
        ]
        if k:
            go(copies(("gz", k), srcs, landing(z, rep), {"fs": lax.rem(fs + 2 * k, n)}))
            return
        go(copies(("gt", 0), srcs, landing(z, rep), twin))
        for i, (s, d) in enumerate(zip(srcs, landing(z, rep))):
            put = pltpu.make_async_copy(s, d, local.at[i])
            put.start()
            puts.append(put)

    def z_step(k):
        refs = landing(origin(k), rep)
        arrived(("gz", k), refs)
        go(copies(("gt", k), refs, refs, twin))

    to_mate(1)
    for s in range(last):
        move(2, s)
    from_mate(1)
    chain(1)
    for s in range(last):
        moved(2, s)

    @pl.loop(0, line)
    def _(t):
        here = block(t, rows, ROWS)
        hidden[here, :] = activations(acts[2, here, :])[3]

    @pl.loop(0, width // wide)
    def _(j):
        cols = block(j, wide, LANES)
        part[0, :, cols] = jnp.dot(
            hidden[...], down[:, cols], preferred_element_type=f32
        ).astype(bf16)

    to_mate(0)
    y_step(order[0])
    from_mate(0)
    chain(0)
    x_step(order[0])
    finish(1)
    y_step(order[1])
    finish(0)
    z_step(order[0])
    x_step(order[1])
    for i in range(2, line):
        y_step(order[i])
        z_step(order[i - 1])
        if i == line - 1:
            outputs()
        x_step(order[i])
    if line == 2:
        outputs()
    for k in order:
        arrived(("gt", k), landing(origin(k), 1 - rep))
    for put in puts:
        put.wait()
    assert len(names) <= send.shape[0]
    for cond, group in pending:

        def drain():
            for copy in group:
                copy.wait_send()

        if cond is None:
            drain()
        else:
            pl.when(cond)(drain)


def fast_shards(n, x_early, x_late, grad_out, w_gate, w_up, w_down, gate_sum, up_sum, down_sum):
    bf16 = jnp.bfloat16
    shape = jax.ShapeDtypeStruct
    line = n // 2
    rows, width = x_early.shape
    hidden_here, depth = w_down.shape
    layer = hidden_here // line
    tokens, half = line * rows, width // 2
    dma, vmem = pltpu.SemaphoreType.DMA, pl.BlockSpec(memory_space=pltpu.VMEM)
    count = 50 * line
    out_late, grad_in, delta_gate, delta_up, delta_down = pl.pallas_call(
        functools.partial(step_kernel, n),
        out_shape=[
            shape((rows, width), bf16),
            shape((rows, width), bf16),
            shape((depth, hidden_here), bf16),
            shape((depth, hidden_here), bf16),
            shape((hidden_here, depth), bf16),
        ],
        in_specs=[vmem, vmem, ANY, ANY, ANY, ANY],
        out_specs=[vmem, vmem, ANY, ANY, ANY],
        scratch_shapes=[
            pltpu.VMEM((3, tokens, width), bf16),
            pltpu.VMEM((width, 2 * layer), bf16),
            pltpu.VMEM((layer, width), bf16),
            pltpu.VMEM((tokens, layer), bf16),
            pltpu.VMEM((tokens, 2 * layer), bf16),
            pltpu.VMEM((2, tokens, width), bf16),
            pltpu.VMEM((2, tokens, half), bf16),
            pltpu.VMEM((2, line, rows, half), bf16),
            pltpu.VMEM((2, line, rows, half), bf16),
            pltpu.VMEM((2, line, rows, half), bf16),
            pltpu.VMEM((width, 2 * layer), bf16),
            pltpu.VMEM((layer, width), bf16),
            pltpu.VMEM((line, depth, 2 * layer), bf16),
            pltpu.VMEM((line, layer, depth), bf16),
            pltpu.VMEM((line, depth // 2, 2 * layer), bf16),
            pltpu.VMEM((line, layer // 2, depth), bf16),
            pltpu.VMEM((2, rows, width), bf16),
            dma((count,)),
            dma((count,)),
            dma((4,)),
        ],
        compiler_params=pltpu.CompilerParams(
            collective_id=0, has_side_effects=True, vmem_limit_bytes=56 * 2**20
        ),
    )(x_early, x_late, grad_out, w_gate, w_up, w_down)
    return (
        out_late,
        grad_in,
        gate_sum + delta_gate.astype(jnp.float32),
        up_sum + delta_up.astype(jnp.float32),
        down_sum + delta_down.astype(jnp.float32),
    )


def shards(x_early, x_late, grad_out, w_gate, w_up, w_down, gate_sum, up_sum, down_sum):
    gate_full, up_full, down_full = (
        lax.all_gather(w_gate, "fs", axis=0, tiled=True),
        lax.all_gather(w_up, "fs", axis=0, tiled=True),
        lax.all_gather(w_down, "fs", axis=1, tiled=True),
    )
    batch_rows = x_early.shape[0]
    stacked = jnp.concatenate([x_early, x_late], axis=0).astype(jnp.float32)
    row_scale = lax.rsqrt(jnp.mean(stacked * stacked, axis=-1, keepdims=True) + epsilon)
    normed = (stacked * row_scale).astype(jnp.bfloat16)
    gate_pre = jnp.dot(normed, gate_full, preferred_element_type=jnp.float32)
    up_pre = jnp.dot(normed, up_full, preferred_element_type=jnp.float32)
    gate_sig = jax.nn.sigmoid(gate_pre)
    hidden = (gate_pre * gate_sig * up_pre).astype(jnp.bfloat16)
    late_part = jnp.dot(hidden[batch_rows:], down_full, preferred_element_type=jnp.float32).astype(
        jnp.bfloat16
    )
    branch = lax.psum(late_part, "tp").astype(jnp.float32)
    out_late = (stacked[batch_rows:] + 0.5 * branch).astype(jnp.bfloat16)
    early_gate = gate_pre[:batch_rows]
    early_upper = up_pre[:batch_rows]
    early_sig = gate_sig[:batch_rows]
    early_hidden = hidden[:batch_rows]
    early_normed = normed[:batch_rows]
    early_scale = row_scale[:batch_rows]
    grad_hidden = 0.5 * contract_cols(grad_out, down_full)
    grad_gate_in = (
        grad_hidden * early_upper * early_sig * (1.0 + early_gate * (1.0 - early_sig))
    ).astype(jnp.bfloat16)
    grad_up_in = (grad_hidden * early_gate * early_sig).astype(jnp.bfloat16)
    normed_part = contract_cols(grad_gate_in, gate_full) + contract_cols(grad_up_in, up_full)
    grad_normed = lax.psum(normed_part.astype(jnp.bfloat16), "tp").astype(jnp.float32)
    unit_rows = stacked[:batch_rows] * early_scale
    inner = jnp.mean(grad_normed * unit_rows, axis=-1, keepdims=True)
    grad_in = (
        grad_out.astype(jnp.float32) + early_scale * (grad_normed - unit_rows * inner)
    ).astype(jnp.bfloat16)
    normed_cols, out_cols = (
        lax.all_to_all(early_normed, "fs", split_axis=1, concat_axis=0, tiled=True),
        lax.all_to_all(grad_out, "fs", split_axis=1, concat_axis=0, tiled=True),
    )
    gate_delta = contract_rows(normed_cols, lax.all_gather(grad_gate_in, "fs", axis=0, tiled=True))
    up_delta = contract_rows(normed_cols, lax.all_gather(grad_up_in, "fs", axis=0, tiled=True))
    down_half = contract_rows(lax.all_gather(early_hidden, "fs", axis=0, tiled=True), out_cols)
    down_delta = 0.5 * down_half
    gate_delta, up_delta, down_delta = (
        lax.psum(gate_delta.astype(jnp.bfloat16), "rep").astype(jnp.float32),
        lax.psum(up_delta.astype(jnp.bfloat16), "rep").astype(jnp.float32),
        lax.psum(down_delta.astype(jnp.bfloat16), "rep").astype(jnp.float32),
    )
    return (out_late, grad_in, gate_sum + gate_delta, up_sum + up_delta, down_sum + down_delta)


def shards_for(mesh):
    n, reps, cores = mesh.shape["fs"], mesh.shape["rep"], mesh.shape["tp"]

    def run(*args):
        rows, width = args[0].shape
        hidden_here, depth = args[5].shape
        line = max(n // 2, 1)
        layer = hidden_here // line
        fits = (
            reps == 2
            and cores == 2
            and n % 2 == 0
            and n >= 4
            and rows % ROWS == 0
            and width % (2 * LANES) == 0
            and depth % (2 * LANES) == 0
            and hidden_here % line == 0
            and layer % LANES == 0
            and layer % (2 * ROWS) == 0
            and 2 * (10 * line * rows * width + 10 * width * layer) < 44 * 2**20
        )
        return fast_shards(n, *args) if fits else shards(*args)

    return run


def solution(mesh):
    placed = (
        P(("rep", "fs"), None),
        P(("rep", "fs"), None),
        P(("rep", "fs"), None),
        P("fs", "tp"),
        P("fs", "tp"),
        P("tp", "fs"),
        P("fs", "tp"),
        P("fs", "tp"),
        P("tp", "fs"),
    )
    return jax.shard_map(
        shards_for(mesh),
        mesh=mesh,
        in_specs=placed,
        out_specs=(
            P(("rep", "fs"), None),
            P(("rep", "fs"), None),
            P("fs", "tp"),
            P("fs", "tp"),
            P("tp", "fs"),
        ),
        check_vma=False,
    )
```

time: 211 us -> 202 us (0.957)
  matrix products: 14.9 us -> 0 us
  Pallas kernels: 182 us -> 192 us
  local copies, waits for them, and re-layouts: 4.4 us -> 1.56 us
    dot_general x7 -> x0, matrix products: 14.9 us -> none  [the longest x3 5.13 us: contract_cols(): lax.dot_general(left, right, (((1,), (1,)), ((), ())), preferred_element_...]
    pallas_call x3 -> x1, Pallas kernels: 182 us -> 192 us  [fast_shards(): pl.pallas_call(functools.partial(step_kernel, n), out_shape=[shape((rows,...]
    add x0 -> x2, other arithmetic: none -> 4.98 us  [the longest x1 3.68 us: fast_shards(): up_sum + delta_up.astype(jnp.float32)]
    reduce_sum x3 -> x0, other arithmetic: 2.84 us -> none  [the longest x2 2.56 us: fast_shards(): jnp.mean(v * v, axis=-1, keepdims=True) + epsilon]
    unnamed x14, local copies, waits for them, and re-layouts: 4.3 us -> 1.56 us
where the time goes in v1:
time: 202 us; the launch traced here: 199 us
  Pallas kernels  192 us (95%)
  other arithmetic  4.98 us (2%)
    pallas_call x1, Pallas kernels, fast_shards(): pl.pallas_call(functools.partial(step_kernel, n), out_shape=[shape((rows,...  192 us

profile of v1, /device:TPU:0, one launch (start us, length us, event | category | flops | bytes accessed | tf_op | source)
XLA Modules:
  0.0 199.4 jit_solution(3460122334776851433)
XLA Ops:
  0.6 0.0 copy-start.2
  0.6 0.0 copy-start.1
  0.7 192.2 %shard_map.128 = (bf16[112,2048]{1,0:T(8,128)(2,1)}, bf16[112,2048]{1,0:T(8,128)(2,1)}, bf16[256,1536]{1,0:T(8,128)(2,1)}, bf16[256,1536]{1,0:T(8,128)(2,1)}, bf16[1536,256]{1,0:T(8,128)(2,1)}) custom-call(bf16[112,2048]{1,0:T(8,128)(2,1)} %x_early.1, bf16[112,2048]{1,0:T(8,128)(2,1)} %x_late.1, bf16[112,2048]{1,0:T(8,128)(2,1)} %grad_out.1, ...), custom_call_target="tpu_custom_call" | custom-call | tf_op jit(solution)/shard_map/pallas_call | solution.py:497
  192.8 0.0 copy-done.2
  192.8 0.0 copy-done.1
  192.8 0.0 copy-start
  192.9 0.0 copy-start.3
  192.9 3.7 %convert_add_fusion.1 = (f32[256,1536]{1,0:T(8,128)}, f32[256,1536]{1,0:T(8,128)}) fusion(f32[256,1536]{1,0:T(8,128)S(1)} %copy-done.1, bf16[256,1536]{1,0:T(8,128)(2,1)} %get-tuple-element.13, f32[256,1536]{1,0:T(8,128)S(1)} %copy-done.2, bf16[256,1536]{1,0:T(8,128)(2,1)} %get-tuple-element.12), kind=kLoop, calls=%fused_computation.1 | loop fusion | flops 1572864 | bytes 7864320 | tf_op jit(solution)/shard_map/add | solution.py:538
  196.6 0.0 copy-done
  196.6 0.0 copy-done.3
  196.6 0.0 copy-start.5
  196.6 0.0 copy-start.4
  196.6 1.3 convert_add_fusion
  197.9 0.0 copy-done.5
  197.9 0.8 copy.16
  198.6 0.0 copy-done.4
  198.6 0.8 copy.17
Async XLA Ops:
  0.6 192.2 %copy-start.2 = (f32[256,1536]{1,0:T(8,128)S(1)}, f32[256,1536]{1,0:T(8,128)}, u32[]{:S(2)}) copy-start(f32[256,1536]{1,0:T(8,128)} %param.15) | copy-start | bytes 4718596
  0.6 192.2 %copy-start.1 = (f32[256,1536]{1,0:T(8,128)S(1)}, f32[256,1536]{1,0:T(8,128)}, u32[]{:S(2)}) copy-start(f32[256,1536]{1,0:T(8,128)} %param.16) | copy-start | bytes 4718596
  192.8 3.7 %copy-start = (f32[1536,256]{1,0:T(8,128)S(1)}, f32[1536,256]{1,0:T(8,128)}, u32[]{:S(2)}) copy-start(f32[1536,256]{1,0:T(8,128)} %param.17) | copy-start | bytes 4718596
  192.9 3.7 %copy-start.3 = (bf16[1536,256]{1,0:T(8,128)(2,1)S(1)}, bf16[1536,256]{1,0:T(8,128)(2,1)}, u32[]{:S(2)}) copy-start(bf16[1536,256]{1,0:T(8,128)(2,1)} %get-tuple-element.14) | copy-start | bytes 2359300
  196.6 1.3 copy-start.5
  196.6 2.1 %copy-start.4 = (bf16[112,2048]{1,0:T(8,128)(2,1)S(1)}, bf16[112,2048]{1,0:T(8,128)(2,1)}, u32[]{:S(2)}) copy-start(bf16[112,2048]{1,0:T(8,128)(2,1)} %get-tuple-element.23) | copy-start | bytes 1376260

commit v2 on v1

--- a/solution.py
+++ b/solution.py
@@ -54,6 +54,15 @@
         at = block(i, ROWS, ROWS)
         total = left[at, :].astype(jnp.float32) + right[at, :].astype(jnp.float32)
         dst[at, :] = total.astype(dst.dtype)
+
+
+def named(f):
+    def g(*args):
+        tags = [str(a) for a in args if isinstance(a, int)]
+        with jax.named_scope("_".join([f.__name__.strip("_")] + tags)):
+            return f(*args)
+
+    return g
 
 
 def scale_of(v):
@@ -182,16 +191,21 @@
         keep.start()
 
     barrier = pltpu.get_barrier_semaphore()
+    enter = jax.named_scope("enter")
+    enter.__enter__()
     peers = [twin, mate, side] + [{"fs": lax.rem(fs + 2 * k, n)} for k in range(1, line)]
     for peer in peers:
         pl.semaphore_signal(barrier, inc=1, device_id=peer, device_id_type=MESH)
     pl.semaphore_wait(barrier, len(peers))
-
-    for k in sorted(range(1, line), key=lambda k: -min(k, line - k)):
-        to = {"fs": lax.rem(fs + 2 * k, n)}
-        go(copies(("wz", k), source3(place(k)), slice3(fs, rep), to))
+    enter.__exit__(None, None, None)
+
+    for d in [1] + list(range(last, 1, -1)):
+        up, low = {"fs": lax.rem(fs + 2 * d, n)}, {"fs": lax.rem(fs + n - 2 * d, n)}
+        go(copies(("wu", d), source3(z + d), slice3(fs, rep), up), z + d < line)
+        go(copies(("wd", d), source3(z - d), slice3(fs, rep), low), z - d >= 0)
     go(copies("wy0", own_source, whole3(fs), side))
 
+    @named
     def normalise(i, x):
         @pl.loop(0, rows // ROWS)
         def _(j):
@@ -210,6 +224,7 @@
         src = grad_out.at[:, mine] if i == 1 and s == 0 else spot(i, z + s)
         go(copies(("down", i, s), [src], [spot(i, z + s)], below), (z + s < line) & (z > 0))
 
+    @named
     def move(i, s):
         under, over = z - 1 - s, z + 1 + s
         pl.when(under >= 0)(lambda: arrived(("up", i, s), [spot(i, under)]))
@@ -221,6 +236,7 @@
             go_down(i, s + 1)
         go(copies(("md", i, s), [spot(i, over)], [spot(i, over)], mate), over < line)
 
+    @named
     def moved(i, s):
         under, over = z - 1 - s, z + 1 + s
         pl.when(under >= 0)(lambda: arrived(("mu", i, s), [spot(i, under, other)]))
@@ -235,30 +251,63 @@
     first(0)
     normalise(2, x_late)
 
-    for k in range(1, line):
-        part2 = slice2(origin(k) * 2 + y, rep)
-        arrived(("wz", k), slice3(origin(k) * 2 + y, rep))
-        go(copies(("wy", k), part2, part2, side))
-        go(copies(("wx", k), part2, part2, twin))
-
-    def pass_on(k):
-        part2 = slice2(origin(k) * 2 + 1 - y, rep)
-        arrived(("wy", k), part2)
-        go(copies(("wxx", k), part2, part2, twin))
-
+    def layers(d):
+        return (("wu", z - d, z - d >= 0), ("wd", z + d, z + d < line))
+
+    def on(cond, f):
+        pl.when(cond)(f)
+
+    @named
+    def weights_in(d):
+        for tag, at_z, cond in layers(d):
+            part2 = slice2(at_z * 2 + y, rep)
+            on(cond, lambda: arrived((tag, d), slice3(at_z * 2 + y, rep)))
+            go(copies((tag, "y", d), part2, part2, side), cond)
+            go(copies((tag, "x", d), part2, part2, twin), cond)
+
+    def turned(d):
+        return d == 2
+
+    @named
+    def relay(d):
+        for tag, at_z, cond in layers(d):
+            if turned(d):
+                part2, key, peer = slice2(at_z * 2 + y, 1 - rep), "x", side
+            else:
+                part2, key, peer = slice2(at_z * 2 + 1 - y, rep), "y", twin
+            on(cond, lambda: arrived((tag, key, d), part2))
+            go(copies((tag, "xy", d), part2, part2, peer), cond)
+
+    @named
+    def weights_done(d):
+        for tag, at_z, cond in layers(d):
+            if turned(d):
+                part2, key = slice2(at_z * 2 + 1 - y, rep), "y"
+            else:
+                part2, key = slice2(at_z * 2 + y, 1 - rep), "x"
+            on(cond, lambda: arrived((tag, key, d), part2))
+            on(cond, lambda: arrived((tag, "xy", d), slice2(at_z * 2 + 1 - y, 1 - rep)))
+
+    weights_in(1)
+    if line > 2:
+        weights_in(last)
     for s in range(last - 1):
+        relay(s + 1 if s == 0 else last + 1 - s)
         move(1, s)
+        if last - 1 - s > 1:
+            weights_in(last - 1 - s)
         move(0, s)
-        pass_on(s + 1)
     first(2)
-    for k in range(max(last, 1), line):
-        pass_on(k)
-    for keep in keeps:
-        keep.wait()
-    arrived("wy0", whole3(fs + 1 - 2 * y))
-    for k in range(1, line):
-        arrived(("wx", k), slice2(origin(k) * 2 + y, 1 - rep))
-        arrived(("wxx", k), slice2(origin(k) * 2 + 1 - y, 1 - rep))
+    if line > 2:
+        relay(2)
+    else:
+        relay(1)
+    with jax.named_scope("weights_wait"):
+        for keep in keeps:
+            keep.wait()
+        arrived("wy0", whole3(fs + 1 - 2 * y))
+    for d in range(1, line):
+        weights_done(d)
 
     def activations(x):
         pre = jnp.dot(x, gate_up[...], preferred_element_type=f32)
@@ -274,18 +323,23 @@
         grads[here, pl.ds(0, layer)] = (grad_hidden * u * s * (1.0 + g * (1.0 - s))).astype(bf16)
         grads[here, pl.ds(layer, layer)] = (grad_hidden * g * s).astype(bf16)
 
-    early_block(z)
+    with jax.named_scope("early_own"):
+        early_block(z)
     for s in range(last):
         if s == last - 1:
+            for earlier in range(last - 2):
+                move(2, earlier)
             move(1, s)
             move(0, s)
         moved(1, s)
         moved(0, s)
 
-        @pl.loop(0, 2)
-        def _(d):
-            to = z + (2 * d - 1) * (s + 1)
-            pl.when((to >= 0) & (to < line))(lambda: early_block(to))
+        with jax.named_scope(f"early_{s}"):
+
+            @pl.loop(0, 2)
+            def _(d):
+                to = z + (2 * d - 1) * (s + 1)
+                pl.when((to >= 0) & (to < line))(lambda: early_block(to))
 
     order = list(range(1, line)) + [0]
 
@@ -304,23 +358,25 @@
 
     for k in order:
         owner = place(k) * 2 + 1 - y
-        weight_grads(owner)
-        go(copies(("gy", k), deltas(owner), [y_gate_up.at[place(k)], y_down.at[place(k)]], side))
-
-    @pl.loop(0, line)
-    def _(t):
-        weight_grads(t * 2 + y)
+        with jax.named_scope(f"wgrad_{k}"):
+            weight_grads(owner)
+        ref_gate_up, ref_down = deltas(owner)
+        go(copies(("gy", 0, k), [ref_down], [y_down.at[place(k)]], side))
+        go(copies(("gy", 1, k), [ref_gate_up], [y_gate_up.at[place(k)]], side))
+
+    with jax.named_scope("wgrad_own"):
+
+        @pl.loop(0, line)
+        def _(t):
+            weight_grads(t * 2 + y)
 
     wide = next(b for b in (512, 256, 128) if width % b == 0)
 
-    @pl.loop(0, width // wide)
-    def _(j):
-        cols = block(j, wide, LANES)
-        part[1, :, cols] = contract_cols(grads[...], gate_up[block(j, wide, ROWS), :]).astype(bf16)
-
+    @named
     def to_mate(i):
         go(copies(("pm", i), [part.at[i, :, other]], [part_in.at[i]], mate))
 
+    @named
     def from_mate(i):
         arrived(("pm", i), [part_in.at[i]])
 
@@ -329,43 +385,35 @@
             here = block(t, rows, ROWS)
             add_strips(sums.at[i, t], part.at[i, here, mine], part_in.at[i, here, :])
 
-    def chain(i):
-        for d in range(last):
-            t = last - d
-
-            def add_up():
-                arrived(("zu", i, t), [from_below.at[i, t]])
-                add_strips(sums.at[i, t], sums.at[i, t], from_below.at[i, t])
-
-            pl.when((z >= 1) & (z < t))(add_up)
-            go(copies(("zu", i, t), [sums.at[i, t]], [from_below.at[i, t]], above), z < t)
-
-            def add_down():
-                arrived(("zd", i, d), [from_above.at[i, d]])
-                add_strips(sums.at[i, d], sums.at[i, d], from_above.at[i, d])
-
-            pl.when((z < last) & (z > d))(add_down)
-            go(copies(("zd", i, d), [sums.at[i, d]], [from_above.at[i, d]], below), z > d)
-
+    def add_in(i, t, key, landed):
+        arrived((key, i, t), [landed.at[i, t]])
+        add_strips(sums.at[i, t], sums.at[i, t], landed.at[i, t])
+
+    @named
+    def chain(i, stage):
+        for here in range(line):
+            up = [("zu", t, here + last - t) for t in range(last, here, -1)]
+            low = [("zd", t, last - here + t) for t in range(here)]
+            for key, t, when in sorted(up + low, key=lambda v: v[2]):
+                first_hop = here == (0 if key == "zu" else last)
+                if stage != (0 if first_hop else when):
+                    continue
+                landed, peer = (from_below, above) if key == "zu" else (from_above, below)
+                if not first_hop:
+                    on(z == here, functools.partial(add_in, i, t, key, landed))
+                go(copies((key, i, t), [sums.at[i, t]], [landed.at[i, t]], peer), z == here)
+
+    @named
     def finish(i):
         for t in range(line):
             if t > 0:
-
-                def add_up():
-                    arrived(("zu", i, t), [from_below.at[i, t]])
-                    add_strips(sums.at[i, t], sums.at[i, t], from_below.at[i, t])
-
-                pl.when(z == t)(add_up)
+                on(z == t, functools.partial(add_in, i, t, "zu", from_below))
             if t < last:
-
-                def add_down():
-                    arrived(("zd", i, t), [from_above.at[i, t]])
-                    add_strips(sums.at[i, t], sums.at[i, t], from_above.at[i, t])
-
-                pl.when(z == t)(add_down)
+                on(z == t, functools.partial(add_in, i, t, "zd", from_above))
         full[i, :, mine] = sums[i, z]
         go(copies(("fm", i), [full.at[i, :, mine]], [full.at[i, :, mine]], mate))
 
+    @named
     def outputs():
         for i in range(2):
             arrived(("fm", i), [full.at[i, :, other]])
@@ -383,105 +431,126 @@
             kept = acts[1, pl.ds(pl.multiple_of(z * rows + j * ROWS, ROWS), ROWS), :].astype(f32)
             grad_in[here, :] = (kept + scale * (grad_normed - unit * inner)).astype(bf16)
 
-    def y_step(k):
+    @named
+    def y_step(k, a):
         t = place(k)
-        arrived(("gy", k), [y_gate_up.at[t], y_down.at[t]])
-        own = deltas(t * 2 + y)
-        add_strips(y_gate_up.at[t], own[0], y_gate_up.at[t])
-        add_strips(y_down.at[t], own[1], y_down.at[t])
-        srcs = [
-            y_gate_up.at[t, block(1 - rep, deep, ROWS), :],
-            y_down.at[t, block(1 - rep, tall, ROWS), :],
-        ]
-        go(copies(("gx", k), srcs, [x_gate_up.at[t], x_down.at[t]], twin))
-
-    def landing(place_of, who):
+        landed, went = (y_gate_up, x_gate_up) if a else (y_down, x_down)
+        arrived(("gy", a, k), [landed.at[t]])
+        add_strips(landed.at[t], deltas(t * 2 + y)[1 - a], landed.at[t])
+        src = landed.at[t, block(1 - rep, deep if a else tall, ROWS), :]
+        go(copies(("gx", a, k), [src], [went.at[t]], twin))
+
+    def landing(place_of, who, a):
         at_rows, at_cols = block(who, deep, ROWS), block(place_of, layer, LANES)
-        return [
-            delta_gate.at[at_rows, at_cols],
-            delta_up.at[at_rows, at_cols],
-            delta_down.at[block(place_of * 2 + who, tall, ROWS), :],
-        ]
+        if a:
+            return [delta_gate.at[at_rows, at_cols], delta_up.at[at_rows, at_cols]]
+        return [delta_down.at[block(place_of * 2 + who, tall, ROWS), :]]
 
     puts = []
 
-    def x_step(k):
+    @named
+    def x_step(k, a):
         t = place(k)
-        arrived(("gx", k), [x_gate_up.at[t], x_down.at[t]])
-        add_strips(x_gate_up.at[t], y_gate_up.at[t, block(rep, deep, ROWS), :], x_gate_up.at[t])
-        add_strips(x_down.at[t], y_down.at[t, block(rep, tall, ROWS), :], x_down.at[t])
-        srcs = [
-            x_gate_up.at[t, :, pl.ds(0, layer)],
-            x_gate_up.at[t, :, pl.ds(layer, layer)],
-            x_down.at[t],
-        ]
+        landed, kept = (x_gate_up, y_gate_up) if a else (x_down, y_down)
+        arrived(("gx", a, k), [landed.at[t]])
+        own = kept.at[t, block(rep, deep if a else tall, ROWS), :]
+        add_strips(landed.at[t], own, landed.at[t])
+        srcs = [landed.at[t]]
+        if a:
+            srcs = [landed.at[t, :, pl.ds(0, layer)], landed.at[t, :, pl.ds(layer, layer)]]
+        to = landing(z, rep, a)
         if k:
-            go(copies(("gz", k), srcs, landing(z, rep), {"fs": lax.rem(fs + 2 * k, n)}))
+            go(copies(("gz", a, k), srcs, to, {"fs": lax.rem(fs + 2 * k, n)}))
             return
-        go(copies(("gt", 0), srcs, landing(z, rep), twin))
-        for i, (s, d) in enumerate(zip(srcs, landing(z, rep))):
-            put = pltpu.make_async_copy(s, d, local.at[i])
+        go(copies(("gt", a, 0), srcs, to, twin))
+        for i, (s, d) in enumerate(zip(srcs, to)):
+            put = pltpu.make_async_copy(s, d, local.at[a + i])
             put.start()
             puts.append(put)
 
-    def z_step(k):
-        refs = landing(origin(k), rep)
-        arrived(("gz", k), refs)
-        go(copies(("gt", k), refs, refs, twin))
+    @named
+    def z_step(k, a):
+        refs = landing(origin(k), rep, a)
+        arrived(("gz", a, k), refs)
+        go(copies(("gt", a, k), refs, refs, twin))
+
+    move(2, max(last - 2, 0))
+    with jax.named_scope("norm_part"):
+
+        @pl.loop(0, width // wide)
+        def _(j):
+            cols = block(j, wide, LANES)
+            product = contract_cols(grads[...], gate_up[block(j, wide, ROWS), :])
+            part[1, :, cols] = product.astype(bf16)
 
     to_mate(1)
-    for s in range(last):
-        move(2, s)
+    y_step(order[0], 0)
     from_mate(1)
-    chain(1)
+    chain(1, 0)
+    if last > 1:
+        move(2, last - 1)
+    y_step(order[0], 1)
+    x_step(order[0], 0)
     for s in range(last):
         moved(2, s)
-
-    @pl.loop(0, line)
-    def _(t):
-        here = block(t, rows, ROWS)
-        hidden[here, :] = activations(acts[2, here, :])[3]
-
-    @pl.loop(0, width // wide)
-    def _(j):
-        cols = block(j, wide, LANES)
-        part[0, :, cols] = jnp.dot(
-            hidden[...], down[:, cols], preferred_element_type=f32
-        ).astype(bf16)
+    with jax.named_scope("late_hidden"):
+
+        @pl.loop(0, line)
+        def _(t):
+            here = block(t, rows, ROWS)
+            hidden[here, :] = activations(acts[2, here, :])[3]
+
+    x_step(order[0], 1)
+    chain(1, 1)
+    with jax.named_scope("late_part"):
+
+        @pl.loop(0, width // wide)
+        def _(j):
+            cols = block(j, wide, LANES)
+            product = jnp.dot(hidden[...], down[:, cols], preferred_element_type=f32)
+            part[0, :, cols] = product.astype(bf16)
 
     to_mate(0)
-    y_step(order[0])
+    for stage in range(2, last):
+        chain(1, stage)
+    y_step(order[1], 0)
     from_mate(0)
-    chain(0)
-    x_step(order[0])
-    finish(1)
-    y_step(order[1])
-    finish(0)
-    z_step(order[0])
-    x_step(order[1])
-    for i in range(2, line):
-        y_step(order[i])
-        z_step(order[i - 1])
-        if i == line - 1:
+    chain(0, 0)
+    y_step(order[1], 1)
+    for i in range(1, line):
+        x_step(order[i], 0)
+        if i == 1:
+            finish(1)
+        if i < last:
+            x_step(order[i], 1)
+            chain(0, i)
+            for a in range(2):
+                y_step(order[i + 1], a)
+        else:
+            finish(0)
+            x_step(order[i], 1)
             outputs()
-        x_step(order[i])
-    if line == 2:
-        outputs()
-    for k in order:
-        arrived(("gt", k), landing(origin(k), 1 - rep))
-    for put in puts:
-        put.wait()
-    assert len(names) <= send.shape[0]
-    for cond, group in pending:
-
-        def drain():
-            for copy in group:
-                copy.wait_send()
-
-        if cond is None:
-            drain()
-        else:
-            pl.when(cond)(drain)
+        for a in range(2):
+            z_step(order[i - 1], a)
+    with jax.named_scope("last_in"):
+        for a in range(2):
+            for k in order:
+                arrived(("gt", a, k), landing(origin(k), 1 - rep, a))
+
+    with jax.named_scope("drain"):
+        for put in puts:
+            put.wait()
+        assert len(names) <= send.shape[0]
+        for cond, group in pending:
+
+            def drain():
+                for copy in group:
+                    copy.wait_send()
+
+            if cond is None:
+                drain()
+            else:
+                pl.when(cond)(drain)
 
 
 def fast_shards(n, x_early, x_late, grad_out, w_gate, w_up, w_down, gate_sum, up_sum, down_sum):
@@ -493,7 +562,7 @@
     layer = hidden_here // line
     tokens, half = line * rows, width // 2
     dma, vmem = pltpu.SemaphoreType.DMA, pl.BlockSpec(memory_space=pltpu.VMEM)
-    count = 50 * line
+    count = 60 * line
     out_late, grad_in, delta_gate, delta_up, delta_down = pl.pallas_call(
         functools.partial(step_kernel, n),
         out_shape=[

time: 202 us -> 157 us (0.78); the launches traced: 199 us -> 157 us
  Pallas kernels: 192 us -> 150 us
    pallas_call x1, Pallas kernels: 192 us -> 150 us  [fast_shards(): pl.pallas_call(functools.partial(step_kernel, n), out_shape=[shape((rows,...]
where the time goes in v2:
time: 157 us
  Pallas kernels  150 us (96%)
  other arithmetic  4.98 us (3%)
    pallas_call x1, Pallas kernels, fast_shards(): pl.pallas_call(functools.partial(step_kernel, n), out_shape=[shape((rows,...  150 us
    add x1, other arithmetic, fast_shards(): up_sum + delta_up.astype(jnp.float32)  3.68 us

profile of v2, /device:TPU:0, one launch (start us, length us, event | category | flops | bytes accessed | tf_op | source)
XLA Modules:
  0.0 156.8 jit_solution(17167662087484202514)
XLA Ops:
  0.6 0.0 copy-start.2
  0.6 0.0 copy-start.1
  0.7 149.6 %shard_map.128 = (bf16[112,2048]{1,0:T(8,128)(2,1)}, bf16[112,2048]{1,0:T(8,128)(2,1)}, bf16[256,1536]{1,0:T(8,128)(2,1)}, bf16[256,1536]{1,0:T(8,128)(2,1)}, bf16[1536,256]{1,0:T(8,128)(2,1)}) custom-call(bf16[112,2048]{1,0:T(8,128)(2,1)} %x_early.1, bf16[112,2048]{1,0:T(8,128)(2,1)} %x_late.1, bf16[112,2048]{1,0:T(8,128)(2,1)} %grad_out.1, ...), custom_call_target="tpu_custom_call" | custom-call | tf_op jit(solution)/shard_map/pallas_call | solution.py:566
  150.2 0.0 copy-done.2
  150.3 0.0 copy-done.1
  150.3 0.0 copy-start
  150.3 0.0 copy-start.3
  150.3 3.7 %convert_add_fusion.1 = (f32[256,1536]{1,0:T(8,128)}, f32[256,1536]{1,0:T(8,128)}) fusion(f32[256,1536]{1,0:T(8,128)S(1)} %copy-done.1, bf16[256,1536]{1,0:T(8,128)(2,1)} %get-tuple-element.13, f32[256,1536]{1,0:T(8,128)S(1)} %copy-done.2, bf16[256,1536]{1,0:T(8,128)(2,1)} %get-tuple-element.12), kind=kLoop, calls=%fused_computation.1 | loop fusion | flops 1572864 | bytes 7864320 | tf_op jit(solution)/shard_map/add | solution.py:607
  154.0 0.0 copy-done
  154.0 0.0 copy-done.3
  154.0 0.0 copy-start.5
  154.0 0.0 copy-start.4
  154.0 1.3 convert_add_fusion
  155.3 0.0 copy-done.5
  155.3 0.8 copy.16
  156.1 0.0 copy-done.4
  156.1 0.8 copy.17
Async XLA Ops:
  0.6 149.6 %copy-start.2 = (f32[256,1536]{1,0:T(8,128)S(1)}, f32[256,1536]{1,0:T(8,128)}, u32[]{:S(2)}) copy-start(f32[256,1536]{1,0:T(8,128)} %param.15) | copy-start | bytes 4718596
  0.6 149.6 %copy-start.1 = (f32[256,1536]{1,0:T(8,128)S(1)}, f32[256,1536]{1,0:T(8,128)}, u32[]{:S(2)}) copy-start(f32[256,1536]{1,0:T(8,128)} %param.16) | copy-start | bytes 4718596
  150.3 3.7 %copy-start = (f32[1536,256]{1,0:T(8,128)S(1)}, f32[1536,256]{1,0:T(8,128)}, u32[]{:S(2)}) copy-start(f32[1536,256]{1,0:T(8,128)} %param.17) | copy-start | bytes 4718596
  150.3 3.7 %copy-start.3 = (bf16[1536,256]{1,0:T(8,128)(2,1)S(1)}, bf16[1536,256]{1,0:T(8,128)(2,1)}, u32[]{:S(2)}) copy-start(bf16[1536,256]{1,0:T(8,128)(2,1)} %get-tuple-element.14) | copy-start | bytes 2359300
  154.0 1.3 copy-start.5
  154.0 2.1 %copy-start.4 = (bf16[112,2048]{1,0:T(8,128)(2,1)S(1)}, bf16[112,2048]{1,0:T(8,128)(2,1)}, u32[]{:S(2)}) copy-start(bf16[112,2048]{1,0:T(8,128)(2,1)} %get-tuple-element.23) | copy-start | bytes 1376260

commit v3 on v2

--- a/solution.py
+++ b/solution.py
@@ -71,8 +71,8 @@
 
 def step_kernel(
     n,
-    x_early,
-    x_late,
+    early_in,
+    late_in,
     grad_out,
     w_gate,
     w_up,
@@ -98,7 +98,11 @@
     y_down,
     x_gate_up,
     x_down,
+    a_gate_up,
+    a_down,
     full,
+    x_early,
+    x_late,
     send,
     recv,
     local,
@@ -115,6 +119,7 @@
     mine, other = block(tp, half, LANES), block(1 - tp, half, LANES)
     names, pending = {}, []
     last = line - 1
+    wide = next(b for b in (512, 256, 128) if half % b == 0)
 
     def at(*key):
         return names.setdefault(key, len(names))
@@ -187,7 +192,11 @@
         for i, (s, d) in enumerate(zip(own_source, whole3(fs)))
     ]
     keeps.append(pltpu.make_async_copy(grad_out, acts.at[1, own_rows, :], local.at[3]))
-    for keep in keeps:
+    loads = [
+        pltpu.make_async_copy(early_in, x_early, local.at[4]),
+        pltpu.make_async_copy(late_in, x_late, local.at[5]),
+    ]
+    for keep in loads + keeps:
         keep.start()
 
     barrier = pltpu.get_barrier_semaphore()
@@ -199,10 +208,12 @@
     pl.semaphore_wait(barrier, len(peers))
     enter.__exit__(None, None, None)
 
-    for d in [1] + list(range(last, 1, -1)):
+    def weights_out(d):
         up, low = {"fs": lax.rem(fs + 2 * d, n)}, {"fs": lax.rem(fs + n - 2 * d, n)}
         go(copies(("wu", d), source3(z + d), slice3(fs, rep), up), z + d < line)
         go(copies(("wd", d), source3(z - d), slice3(fs, rep), low), z - d >= 0)
+
+    weights_out(1)
     go(copies("wy0", own_source, whole3(fs), side))
 
     @named
@@ -246,9 +257,9 @@
         go_up(i, 0)
         go_down(i, 0)
 
-    first(1)
+    for load in loads:
+        load.wait()
     normalise(0, x_early)
-    first(0)
     normalise(2, x_late)
 
     def layers(d):
@@ -289,19 +300,23 @@
             on(cond, lambda: arrived((tag, "xy", d), slice2(at_z * 2 + 1 - y, 1 - rep)))
 
     weights_in(1)
+    for d in range(last, 1, -1):
+        weights_out(d)
+    first(1)
+    first(0)
+    for d in range(last, 2, -1):
+        weights_in(d)
+    relay(1)
     if line > 2:
-        weights_in(last)
+        weights_in(2)
+    for d in range(3, line):
+        relay(d)
     for s in range(last - 1):
-        relay(s + 1 if s == 0 else last + 1 - s)
         move(1, s)
-        if last - 1 - s > 1:
-            weights_in(last - 1 - s)
         move(0, s)
+        if s == 0:
+            relay(2)
     first(2)
-    if line > 2:
-        relay(2)
-    else:
-        relay(1)
     with jax.named_scope("weights_wait"):
         for keep in keeps:
             keep.wait()
@@ -327,8 +342,6 @@
         early_block(z)
     for s in range(last):
         if s == last - 1:
-            for earlier in range(last - 2):
-                move(2, earlier)
             move(1, s)
             move(0, s)
         moved(1, s)
@@ -356,21 +369,54 @@
             down_delta.at[:, block(owner, depth, LANES)],
         ]
 
-    for k in order:
+    lead = order[0]
+    lead_z = place(lead)
+
+    def lead_rows(who):
+        return [
+            gate_up_delta.at[block((lead_z * 2 + v) * 2 + who, deep, ROWS), :] for v in range(2)
+        ]
+
+    def lead_cols(who):
+        return down_delta.at[block(who, tall, ROWS), block(lead_z, 2 * depth, LANES)]
+
+    def y_send(k, a):
+        src = deltas(place(k) * 2 + 1 - y)[1 - a]
+        to = (y_gate_up if a else y_down).at[place(k)]
+        go(copies(("gy", a, k), [src], [to], side))
+
+    with jax.named_scope("wgrad_lead"):
+        for v in range(2):
+            weight_grads(lead_z * 2 + v)
+    go(copies(("ax", 0), [lead_cols(1 - rep)], [a_down], twin))
+    go(copies(("ax", 1), lead_rows(1 - rep), [a_gate_up.at[v] for v in range(2)], twin))
+    for k in order[1:]:
         owner = place(k) * 2 + 1 - y
         with jax.named_scope(f"wgrad_{k}"):
             weight_grads(owner)
-        ref_gate_up, ref_down = deltas(owner)
-        go(copies(("gy", 0, k), [ref_down], [y_down.at[place(k)]], side))
-        go(copies(("gy", 1, k), [ref_gate_up], [y_gate_up.at[place(k)]], side))
-
-    with jax.named_scope("wgrad_own"):
-
-        @pl.loop(0, line)
-        def _(t):
-            weight_grads(t * 2 + y)
-
-    wide = next(b for b in (512, 256, 128) if width % b == 0)
+        if k == order[1]:
+            y_send(k, 0)
+            y_send(k, 1)
+
+    @named
+    def lead_x(a):
+        if a:
+            arrived(("ax", 1), [a_gate_up.at[v] for v in range(2)])
+            for v, own in enumerate(lead_rows(rep)):
+                add_strips(a_gate_up.at[v], own, a_gate_up.at[v])
+            go(copies(("ay", 1), [a_gate_up.at[1 - y]], [x_gate_up.at[lead_z]], side))
+            for k in order[2:3]:
+                y_send(k, 1)
+            for k in order[3:]:
+                y_send(k, 0)
+                y_send(k, 1)
+        else:
+            arrived(("ax", 0), [a_down])
+            add_strips(a_down, lead_cols(rep), a_down)
+            src = a_down.at[:, block(1 - y, depth, LANES)]
+            go(copies(("ay", 0), [src], [x_down.at[lead_z]], side))
+            for k in order[2:3]:
+                y_send(k, 0)
 
     @named
     def to_mate(i):
@@ -396,7 +442,7 @@
             low = [("zd", t, last - here + t) for t in range(here)]
             for key, t, when in sorted(up + low, key=lambda v: v[2]):
                 first_hop = here == (0 if key == "zu" else last)
-                if stage != (0 if first_hop else when):
+                if stage != (max(when - 1, 0) if first_hop else when):
                     continue
                 landed, peer = (from_below, above) if key == "zu" else (from_above, below)
                 if not first_hop:
@@ -414,22 +460,23 @@
         go(copies(("fm", i), [full.at[i, :, mine]], [full.at[i, :, mine]], mate))
 
     @named
-    def outputs():
-        for i in range(2):
-            arrived(("fm", i), [full.at[i, :, other]])
+    def output(i):
+        arrived(("fm", i), [full.at[i, :, other]])
 
         @pl.loop(0, rows // ROWS)
         def _(j):
             here = block(j, ROWS, ROWS)
-            late = x_late[here, :].astype(f32)
-            out_late[here, :] = (late + 0.5 * full[0, here, :].astype(f32)).astype(bf16)
+            total = full[i, here, :].astype(f32)
+            if i == 0:
+                late = x_late[here, :].astype(f32)
+                out_late[here, :] = (late + 0.5 * total).astype(bf16)
+                return
             early = x_early[here, :].astype(f32)
             scale = scale_of(early)
             unit = early * scale
-            grad_normed = full[1, here, :].astype(f32)
-            inner = jnp.mean(grad_normed * unit, axis=-1, keepdims=True)
+            inner = jnp.mean(total * unit, axis=-1, keepdims=True)
             kept = acts[1, pl.ds(pl.multiple_of(z * rows + j * ROWS, ROWS), ROWS), :].astype(f32)
-            grad_in[here, :] = (kept + scale * (grad_normed - unit * inner)).astype(bf16)
+            grad_in[here, :] = (kept + scale * (total - unit * inner)).astype(bf16)
 
     @named
     def y_step(k, a):
@@ -452,8 +499,12 @@
     def x_step(k, a):
         t = place(k)
         landed, kept = (x_gate_up, y_gate_up) if a else (x_down, y_down)
-        arrived(("gx", a, k), [landed.at[t]])
-        own = kept.at[t, block(rep, deep if a else tall, ROWS), :]
+        if k == lead:
+            arrived(("ay", a), [landed.at[t]])
+            own = a_gate_up.at[y] if a else a_down.at[:, block(y, depth, LANES)]
+        else:
+            arrived(("gx", a, k), [landed.at[t]])
+            own = kept.at[t, block(rep, deep if a else tall, ROWS), :]
         add_strips(landed.at[t], own, landed.at[t])
         srcs = [landed.at[t]]
         if a:
@@ -474,64 +525,75 @@
         arrived(("gz", a, k), refs)
         go(copies(("gt", a, k), refs, refs, twin))
 
-    move(2, max(last - 2, 0))
-    with jax.named_scope("norm_part"):
-
-        @pl.loop(0, width // wide)
+    def columns(i, who):
+        @pl.loop(0, half // wide)
         def _(j):
-            cols = block(j, wide, LANES)
-            product = contract_cols(grads[...], gate_up[block(j, wide, ROWS), :])
-            part[1, :, cols] = product.astype(bf16)
-
-    to_mate(1)
-    y_step(order[0], 0)
-    from_mate(1)
-    chain(1, 0)
-    if last > 1:
-        move(2, last - 1)
-    y_step(order[0], 1)
-    x_step(order[0], 0)
-    for s in range(last):
-        moved(2, s)
-    with jax.named_scope("late_hidden"):
+            cols = block(who * (half // wide) + j, wide, LANES)
+            if i:
+                at_rows = block(who * (half // wide) + j, wide, ROWS)
+                product = contract_cols(grads[...], gate_up[at_rows, :])
+            else:
+                product = jnp.dot(hidden[...], down[:, cols], preferred_element_type=f32)
+            part[i, :, cols] = product.astype(bf16)
+
+    @named
+    def partials(i):
+        columns(i, 1 - tp)
+        to_mate(i)
+        columns(i, tp)
+
+    @named
+    def late_hidden():
+        for s in range(last):
+            moved(2, s)
 
         @pl.loop(0, line)
         def _(t):
             here = block(t, rows, ROWS)
             hidden[here, :] = activations(acts[2, here, :])[3]
 
-    x_step(order[0], 1)
-    chain(1, 1)
-    with jax.named_scope("late_part"):
-
-        @pl.loop(0, width // wide)
-        def _(j):
-            cols = block(j, wide, LANES)
-            product = jnp.dot(hidden[...], down[:, cols], preferred_element_type=f32)
-            part[0, :, cols] = product.astype(bf16)
-
-    to_mate(0)
-    for stage in range(2, last):
-        chain(1, stage)
-    y_step(order[1], 0)
-    from_mate(0)
-    chain(0, 0)
-    y_step(order[1], 1)
-    for i in range(1, line):
-        x_step(order[i], 0)
-        if i == 1:
-            finish(1)
-        if i < last:
-            x_step(order[i], 1)
-            chain(0, i)
-            for a in range(2):
-                y_step(order[i + 1], a)
+    for s in range(last - 2):
+        move(2, s)
+    partials(1)
+    @named
+    def wgrad_own():
+        for k in order[1:]:
+            weight_grads(place(k) * 2 + y)
+
+    plan = ["a0", "w", "y20", "m", "c10", "v", "a1", "y21", "h", "x20", "x10", "c11", "p", "x21"]
+    plan += ["y30", "n", "c00", "x11", "z10", "z20", "c12", "x30", "y31", "y00", "c01", "x31"]
+    plan += ["z21", "f1", "x00", "y01", "z30", "c02", "z11", "x01", "o1", "z31", "f0", "o0"]
+    if line != 4:
+        plan = ["w", "m", "v", "h", "p", "n", "a0", "a1"]
+        plan += [f"c{i}{stage}" for i in (1, 0) for stage in range(last)]
+        plan += [f"y{k}{a}" for k in order[1:] for a in (0, 1)]
+        plan += [f"{step}{k}{a}" for k in order for step in "xz" for a in (0, 1) if k or step < "z"]
+        plan += ["f1", "f0", "o1", "o0"]
+    steps = {"y": y_step, "x": x_step, "z": z_step, "c": chain}
+    single = {
+        "a0": lambda: lead_x(0),
+        "a1": lambda: lead_x(1),
+        "w": wgrad_own,
+        "m": lambda: from_mate(1),
+        "n": lambda: from_mate(0),
+        "h": late_hidden,
+        "p": lambda: partials(0),
+        "f1": lambda: finish(1),
+        "f0": lambda: finish(0),
+        "o1": lambda: output(1),
+        "o0": lambda: output(0),
+    }
+
+    def late_moves():
+        for s in range(max(last - 2, 0), last):
+            move(2, s)
+
+    single["v"] = late_moves
+    for name in plan:
+        if name in single:
+            single[name]()
         else:
-            finish(0)
-            x_step(order[i], 1)
-            outputs()
-        for a in range(2):
-            z_step(order[i - 1], a)
+            steps[name[0]](int(name[1]), int(name[2:]))
     with jax.named_scope("last_in"):
         for a in range(2):
             for k in order:
@@ -572,7 +634,7 @@
             shape((depth, hidden_here), bf16),
             shape((hidden_here, depth), bf16),
         ],
-        in_specs=[vmem, vmem, ANY, ANY, ANY, ANY],
+        in_specs=[pl.BlockSpec(memory_space=pltpu.HBM)] * 6,
         out_specs=[vmem, vmem, ANY, ANY, ANY],
         scratch_shapes=[
             pltpu.VMEM((3, tokens, width), bf16),
@@ -591,13 +653,17 @@
             pltpu.VMEM((line, layer, depth), bf16),
             pltpu.VMEM((line, depth // 2, 2 * layer), bf16),
             pltpu.VMEM((line, layer // 2, depth), bf16),
+            pltpu.VMEM((2, depth // 2, 2 * layer), bf16),
+            pltpu.VMEM((layer // 2, 2 * depth), bf16),
             pltpu.VMEM((2, rows, width), bf16),
+            pltpu.VMEM((rows, width), bf16),
+            pltpu.VMEM((rows, width), bf16),
             dma((count,)),
             dma((count,)),
-            dma((4,)),
+            dma((6,)),
         ],
         compiler_params=pltpu.CompilerParams(
-            collective_id=0, has_side_effects=True, vmem_limit_bytes=56 * 2**20
+            collective_id=0, has_side_effects=True, vmem_limit_bytes=60 * 2**20
         ),
     )(x_early, x_late, grad_out, w_gate, w_up, w_down)
     return (

time: 157 us -> 144 us (0.917)
  Pallas kernels: 150 us -> 136 us
    pallas_call x1, Pallas kernels: 150 us -> 136 us  [fast_shards(): pl.pallas_call(functools.partial(step_kernel, n), out_shape=[shape((rows,...]
where the time goes in v3:
time: 144 us
  Pallas kernels  136 us (94%)
  other arithmetic  4.98 us (3%)
  local copies, waits for them, and re-layouts  1.56 us (1%)
    pallas_call x1, Pallas kernels, fast_shards(): pl.pallas_call(functools.partial(step_kernel, n), out_shape=[shape((rows,...  136 us
    add x1, other arithmetic, fast_shards(): up_sum + delta_up.astype(jnp.float32)  3.68 us

profile of v3, /device:TPU:0, one launch (start us, length us, event | category | flops | bytes accessed | tf_op | source)
XLA Modules:
  0.0 143.7 jit_solution(4132850201805693776)
XLA Ops:
  0.6 0.0 copy-start.2
  0.6 0.0 copy-start.1
  0.7 136.5 %shard_map.128 = (bf16[112,2048]{1,0:T(8,128)(2,1)}, bf16[112,2048]{1,0:T(8,128)(2,1)}, bf16[256,1536]{1,0:T(8,128)(2,1)}, bf16[256,1536]{1,0:T(8,128)(2,1)}, bf16[1536,256]{1,0:T(8,128)(2,1)}) custom-call(bf16[112,2048]{1,0:T(8,128)(2,1)} %early_in.1, bf16[112,2048]{1,0:T(8,128)(2,1)} %late_in.1, bf16[112,2048]{1,0:T(8,128)(2,1)} %grad_out.1, ...), custom_call_target="tpu_custom_call" | custom-call | tf_op jit(solution)/shard_map/pallas_call | solution.py:628
  137.1 0.0 copy-done.2
  137.1 0.0 copy-done.1
  137.2 0.0 copy-start
  137.2 0.0 copy-start.3
  137.2 3.7 %convert_add_fusion.1 = (f32[256,1536]{1,0:T(8,128)}, f32[256,1536]{1,0:T(8,128)}) fusion(f32[256,1536]{1,0:T(8,128)S(1)} %copy-done.1, bf16[256,1536]{1,0:T(8,128)(2,1)} %get-tuple-element.13, f32[256,1536]{1,0:T(8,128)S(1)} %copy-done.2, bf16[256,1536]{1,0:T(8,128)(2,1)} %get-tuple-element.12), kind=kLoop, calls=%fused_computation.1 | loop fusion | flops 1572864 | bytes 7864320 | tf_op jit(solution)/shard_map/add | solution.py:673
  140.9 0.0 copy-done
  140.9 0.0 copy-done.3
  140.9 0.0 copy-start.5
  140.9 0.0 copy-start.4
  140.9 1.3 convert_add_fusion
  142.2 0.0 copy-done.5
  142.2 0.8 copy.16
  142.9 0.0 copy-done.4
  142.9 0.8 copy.17
Async XLA Ops:
  0.6 136.5 %copy-start.2 = (f32[256,1536]{1,0:T(8,128)S(1)}, f32[256,1536]{1,0:T(8,128)}, u32[]{:S(2)}) copy-start(f32[256,1536]{1,0:T(8,128)} %param.15) | copy-start | bytes 4718596
  0.6 136.5 %copy-start.1 = (f32[256,1536]{1,0:T(8,128)S(1)}, f32[256,1536]{1,0:T(8,128)}, u32[]{:S(2)}) copy-start(f32[256,1536]{1,0:T(8,128)} %param.16) | copy-start | bytes 4718596
  137.2 3.7 %copy-start = (f32[1536,256]{1,0:T(8,128)S(1)}, f32[1536,256]{1,0:T(8,128)}, u32[]{:S(2)}) copy-start(f32[1536,256]{1,0:T(8,128)} %param.17) | copy-start | bytes 4718596
  137.2 3.7 %copy-start.3 = (bf16[1536,256]{1,0:T(8,128)(2,1)S(1)}, bf16[1536,256]{1,0:T(8,128)(2,1)}, u32[]{:S(2)}) copy-start(bf16[1536,256]{1,0:T(8,128)(2,1)} %get-tuple-element.14) | copy-start | bytes 2359300
  140.9 1.3 copy-start.5
  140.9 2.1 %copy-start.4 = (bf16[112,2048]{1,0:T(8,128)(2,1)S(1)}, bf16[112,2048]{1,0:T(8,128)(2,1)}, u32[]{:S(2)}) copy-start(bf16[112,2048]{1,0:T(8,128)(2,1)} %get-tuple-element.23) | copy-start | bytes 1376260

commit v4 on v3

--- a/solution.py
+++ b/solution.py
@@ -117,22 +117,34 @@
     layer, depth = down.shape[0], w_gate.shape[0]
     half, deep, tall = width // 2, depth // 2, layer // 2
     mine, other = block(tp, half, LANES), block(1 - tp, half, LANES)
-    names, pending = {}, []
+    names, pending, free, made = {}, [], [], []
     last = line - 1
     wide = next(b for b in (512, 256, 128) if half % b == 0)
 
     def at(*key):
         return names.setdefault(key, len(names))
 
+    def send_index():
+        if not free:
+            made.append(len(made))
+            return made[-1]
+        return free.pop()
+
+    def bytes_of(refs):
+        if len(refs) == 1:
+            return refs[0]
+        total = sum(ref.shape[0] * ref.shape[1] for ref in refs)
+        assert total % (2 * layer * ROWS) == 0
+        return gate_up.at[pl.ds(0, total // (2 * layer)), :]
+
     def copies(key, srcs, dsts, peer):
-        return [
-            push(s, d, send.at[at(key, i)], recv.at[at(key, i)], peer)
-            for i, (s, d) in enumerate(zip(srcs, dsts))
-        ]
+        index = send_index()
+        sems = send.at[index], recv.at[at(key)]
+        return index, [push(s, d, *sems, peer) for s, d in zip(srcs, dsts)], bytes_of(dsts)
 
     def go(group, cond=None):
         def start():
-            for copy in group:
+            for copy in group[1]:
                 copy.start()
 
         pending.append((cond, group))
@@ -141,9 +153,20 @@
         else:
             pl.when(cond)(start)
 
+    def drain(groups):
+        for cond, (index, _, ref) in groups:
+
+            def wait():
+                push(ref, ref, send.at[index], recv.at[0], twin).wait_send()
+
+            if cond is None:
+                wait()
+            else:
+                pl.when(cond)(wait)
+
     def arrived(key, refs):
-        for copy in copies(key, refs, refs, twin):
-            copy.wait_recv()
+        ref = bytes_of(refs)
+        push(ref, ref, send.at[0], recv.at[at(key)], twin).wait_recv()
 
     def place(k):
         return lax.rem(z + k, line)
@@ -306,9 +329,9 @@
     first(0)
     for d in range(last, 2, -1):
         weights_in(d)
-    relay(1)
     if line > 2:
         weights_in(2)
+    relay(1)
     for d in range(3, line):
         relay(d)
     for s in range(last - 1):
@@ -316,6 +339,7 @@
         move(0, s)
         if s == 0:
             relay(2)
+    early_count = len(pending)
     first(2)
     with jax.named_scope("weights_wait"):
         for keep in keeps:
@@ -442,7 +466,7 @@
             low = [("zd", t, last - here + t) for t in range(here)]
             for key, t, when in sorted(up + low, key=lambda v: v[2]):
                 first_hop = here == (0 if key == "zu" else last)
-                if stage != (max(when - 1, 0) if first_hop else when):
+                if stage != when:
                     continue
                 landed, peer = (from_below, above) if key == "zu" else (from_above, below)
                 if not first_hop:
@@ -555,6 +579,11 @@
     for s in range(last - 2):
         move(2, s)
     partials(1)
+    with jax.named_scope("recycle"):
+        drain(pending[:early_count])
+        free.extend(group[0] for _, group in pending[:early_count])
+        del pending[:early_count]
+
     @named
     def wgrad_own():
         for k in order[1:]:
@@ -562,7 +591,7 @@
 
     plan = ["a0", "w", "y20", "m", "c10", "v", "a1", "y21", "h", "x20", "x10", "c11", "p", "x21"]
     plan += ["y30", "n", "c00", "x11", "z10", "z20", "c12", "x30", "y31", "y00", "c01", "x31"]
-    plan += ["z21", "f1", "x00", "y01", "z30", "c02", "z11", "x01", "o1", "z31", "f0", "o0"]
+    plan += ["z21", "x00", "y01", "z11", "z30", "f1", "x01", "c02", "z31", "o1", "f0", "o0"]
     if line != 4:
         plan = ["w", "m", "v", "h", "p", "n", "a0", "a1"]
         plan += [f"c{i}{stage}" for i in (1, 0) for stage in range(last)]
@@ -602,17 +631,8 @@
     with jax.named_scope("drain"):
         for put in puts:
             put.wait()
-        assert len(names) <= send.shape[0]
-        for cond, group in pending:
-
-            def drain():
-                for copy in group:
-                    copy.wait_send()
-
-            if cond is None:
-                drain()
-            else:
-                pl.when(cond)(drain)
+        assert len(names) <= recv.shape[0] and len(made) <= send.shape[0]
+        drain(pending)
 
 
 def fast_shards(n, x_early, x_late, grad_out, w_gate, w_up, w_down, gate_sum, up_sum, down_sum):
@@ -624,7 +644,6 @@
     layer = hidden_here // line
     tokens, half = line * rows, width // 2
     dma, vmem = pltpu.SemaphoreType.DMA, pl.BlockSpec(memory_space=pltpu.VMEM)
-    count = 60 * line
     out_late, grad_in, delta_gate, delta_up, delta_down = pl.pallas_call(
         functools.partial(step_kernel, n),
         out_shape=[
@@ -658,8 +677,8 @@
             pltpu.VMEM((2, rows, width), bf16),
             pltpu.VMEM((rows, width), bf16),
             pltpu.VMEM((rows, width), bf16),
-            dma((count,)),
-            dma((count,)),
+            dma((22 * line - 14,)),
+            dma((32 * line - 21,)),
             dma((6,)),
         ],
         compiler_params=pltpu.CompilerParams(

time: 144 us -> 141 us (0.979)
  Pallas kernels: 136 us -> 134 us
    pallas_call x1, Pallas kernels: 136 us -> 134 us  [fast_shards(): pl.pallas_call(functools.partial(step_kernel, n), out_shape=[shape((rows,...]
where the time goes in v4:
time: 141 us
  Pallas kernels  134 us (95%)
  other arithmetic  4.98 us (4%)
  local copies, waits for them, and re-layouts  1.56 us (1%)
    pallas_call x1, Pallas kernels, fast_shards(): pl.pallas_call(functools.partial(step_kernel, n), out_shape=[shape((rows,...  134 us
    add x1, other arithmetic, fast_shards(): up_sum + delta_up.astype(jnp.float32)  3.68 us

profile of v4, /device:TPU:0, one launch (start us, length us, event | category | flops | bytes accessed | tf_op | source)
XLA Modules:
  0.0 141.1 jit_solution(10055691933671672090)
XLA Ops:
  0.6 0.0 copy-start.2
  0.6 0.0 copy-start.1
  0.7 133.8 %shard_map.128 = (bf16[112,2048]{1,0:T(8,128)(2,1)}, bf16[112,2048]{1,0:T(8,128)(2,1)}, bf16[256,1536]{1,0:T(8,128)(2,1)}, bf16[256,1536]{1,0:T(8,128)(2,1)}, bf16[1536,256]{1,0:T(8,128)(2,1)}) custom-call(bf16[112,2048]{1,0:T(8,128)(2,1)} %early_in.1, bf16[112,2048]{1,0:T(8,128)(2,1)} %late_in.1, bf16[112,2048]{1,0:T(8,128)(2,1)} %grad_out.1, ...), custom_call_target="tpu_custom_call" | custom-call | tf_op jit(solution)/shard_map/pallas_call | solution.py:647
  134.5 0.0 copy-done.2
  134.5 0.0 copy-done.1
  134.5 0.0 copy-start
  134.5 0.0 copy-start.3
  134.5 3.7 %convert_add_fusion.1 = (f32[256,1536]{1,0:T(8,128)}, f32[256,1536]{1,0:T(8,128)}) fusion(f32[256,1536]{1,0:T(8,128)S(1)} %copy-done.1, bf16[256,1536]{1,0:T(8,128)(2,1)} %get-tuple-element.13, f32[256,1536]{1,0:T(8,128)S(1)} %copy-done.2, bf16[256,1536]{1,0:T(8,128)(2,1)} %get-tuple-element.12), kind=kLoop, calls=%fused_computation.1 | loop fusion | flops 1572864 | bytes 7864320 | tf_op jit(solution)/shard_map/add | solution.py:692
  138.2 0.0 copy-done
  138.2 0.0 copy-done.3
  138.2 0.0 copy-start.5
  138.2 0.0 copy-start.4
  138.2 1.3 convert_add_fusion
  139.5 0.0 copy-done.5
  139.5 0.8 copy.16
  140.3 0.0 copy-done.4
  140.3 0.8 copy.17
Async XLA Ops:
  0.6 133.9 %copy-start.2 = (f32[256,1536]{1,0:T(8,128)S(1)}, f32[256,1536]{1,0:T(8,128)}, u32[]{:S(2)}) copy-start(f32[256,1536]{1,0:T(8,128)} %param.15) | copy-start | bytes 4718596
  0.6 133.9 %copy-start.1 = (f32[256,1536]{1,0:T(8,128)S(1)}, f32[256,1536]{1,0:T(8,128)}, u32[]{:S(2)}) copy-start(f32[256,1536]{1,0:T(8,128)} %param.16) | copy-start | bytes 4718596
  134.5 3.7 %copy-start = (f32[1536,256]{1,0:T(8,128)S(1)}, f32[1536,256]{1,0:T(8,128)}, u32[]{:S(2)}) copy-start(f32[1536,256]{1,0:T(8,128)} %param.17) | copy-start | bytes 4718596
  134.5 3.7 %copy-start.3 = (bf16[1536,256]{1,0:T(8,128)(2,1)S(1)}, bf16[1536,256]{1,0:T(8,128)(2,1)}, u32[]{:S(2)}) copy-start(bf16[1536,256]{1,0:T(8,128)(2,1)} %get-tuple-element.14) | copy-start | bytes 2359300
  138.2 1.3 copy-start.5
  138.2 2.1 %copy-start.4 = (bf16[112,2048]{1,0:T(8,128)(2,1)S(1)}, bf16[112,2048]{1,0:T(8,128)(2,1)}, u32[]{:S(2)}) copy-start(bf16[112,2048]{1,0:T(8,128)(2,1)} %get-tuple-element.23) | copy-start | bytes 1376260

commit v5 on v4

--- a/solution.py
+++ b/solution.py
@@ -591,7 +591,7 @@
 
     plan = ["a0", "w", "y20", "m", "c10", "v", "a1", "y21", "h", "x20", "x10", "c11", "p", "x21"]
     plan += ["y30", "n", "c00", "x11", "z10", "z20", "c12", "x30", "y31", "y00", "c01", "x31"]
-    plan += ["z21", "x00", "y01", "z11", "z30", "f1", "x01", "c02", "z31", "o1", "f0", "o0"]
+    plan += ["z21", "x00", "z11", "y01", "z30", "x01", "f1", "c02", "z31", "o1", "f0", "o0"]
     if line != 4:
         plan = ["w", "m", "v", "h", "p", "n", "a0", "a1"]
         plan += [f"c{i}{stage}" for i in (1, 0) for stage in range(last)]
@@ -685,13 +685,61 @@
             collective_id=0, has_side_effects=True, vmem_limit_bytes=60 * 2**20
         ),
     )(x_early, x_late, grad_out, w_gate, w_up, w_down)
-    return (
-        out_late,
-        grad_in,
-        gate_sum + delta_gate.astype(jnp.float32),
-        up_sum + delta_up.astype(jnp.float32),
-        down_sum + delta_down.astype(jnp.float32),
-    )
+    out_late, grad_in, new_gate, new_up, new_down = settle(
+        out_late, grad_in, gate_sum, up_sum, down_sum, delta_gate, delta_up, delta_down
+    )
+    return out_late, grad_in, new_gate, new_up, new_down
+
+
+PARTS = 2
+
+
+def settle_kernel(*refs):
+    ins, outs, held, sem = refs[:8], refs[8:13], refs[13:21], refs[21]
+    loads = [pltpu.make_async_copy(ins[i], held[i], sem.at[i]) for i in range(8)]
+    for i in (2, 5, 3, 6, 4, 7, 0, 1):
+        loads[i].start()
+    stores = []
+
+    def store(src, dst):
+        copy = pltpu.make_async_copy(src, dst, sem.at[8 + len(stores)])
+        copy.start()
+        stores.append(copy)
+
+    for i in range(2, 5):
+        loads[i].wait()
+        loads[i + 3].wait()
+        total, delta = held[i], held[i + 3]
+        size = total.shape[0] // PARTS
+        for p in range(PARTS):
+
+            @pl.loop(0, size // ROWS)
+            def _(j):
+                at = pl.ds(pl.multiple_of(p * size + j * ROWS, ROWS), ROWS)
+                total[at, :] = total[at, :] + delta[at, :].astype(jnp.float32)
+
+            at = pl.ds(p * size, size)
+            store(total.at[at, :], outs[i].at[at, :])
+        if i == 2:
+            for k in range(2):
+                loads[k].wait()
+                store(held[k], outs[k])
+    for copy in stores:
+        copy.wait()
+
+
+def settle(*args):
+    outs = [jax.ShapeDtypeStruct(v.shape, v.dtype) for v in args[:5]]
+    size = sum(v.size for v in args[2:5])
+    return pl.pallas_call(
+        settle_kernel,
+        out_shape=outs,
+        in_specs=[ANY] * 8,
+        out_specs=[ANY] * 5,
+        scratch_shapes=[pltpu.VMEM(v.shape, v.dtype) for v in args]
+        + [pltpu.SemaphoreType.DMA((10 + 3 * PARTS,))],
+        cost_estimate=pl.CostEstimate(flops=size, bytes_accessed=10 * size, transcendentals=0),
+    )(*args)
 
 
 def shards(x_early, x_late, grad_out, w_gate, w_up, w_down, gate_sum, up_sum, down_sum):

time: 141 us -> 140 us (level)
  Pallas kernels: 134 us -> 139 us
  other arithmetic: 4.98 us -> 0 us
  local copies, waits for them, and re-layouts: 1.56 us -> 0 us
    pallas_call x0 -> x1, Pallas kernels: none -> 5.78 us  [settle(): pl.pallas_call(settle_kernel, out_shape=outs, in_specs=[ANY] * 8, out_spe...]
    add x2 -> x0, other arithmetic: 4.98 us -> none  [the longest x1 3.68 us: fast_shards(): up_sum + delta_up.astype(jnp.float32)]
    unnamed x14 -> x0, local copies, waits for them, and re-layouts: 1.56 us -> none
where the time goes in v5:
time: 140 us
  Pallas kernels  139 us (99%)
    pallas_call x1, Pallas kernels, fast_shards(): pl.pallas_call(functools.partial(step_kernel, n), out_shape=[shape((rows,...  133 us
    pallas_call x1, Pallas kernels, settle(): pl.pallas_call(settle_kernel, out_shape=outs, in_specs=[ANY] * 8, out_spe...  5.78 us

profile of v5, /device:TPU:0, one launch (start us, length us, event | category | flops | bytes accessed | tf_op | source)
XLA Modules:
  0.0 139.9 jit_solution(7296617646299902739)
XLA Ops:
  0.6 133.5 %shard_map.128 = (bf16[112,2048]{1,0:T(8,128)(2,1)}, bf16[112,2048]{1,0:T(8,128)(2,1)}, bf16[256,1536]{1,0:T(8,128)(2,1)}, bf16[256,1536]{1,0:T(8,128)(2,1)}, bf16[1536,256]{1,0:T(8,128)(2,1)}) custom-call(bf16[112,2048]{1,0:T(8,128)(2,1)} %early_in.1, bf16[112,2048]{1,0:T(8,128)(2,1)} %late_in.1, bf16[112,2048]{1,0:T(8,128)(2,1)} %grad_out.1, ...), custom_call_target="tpu_custom_call" | custom-call | tf_op jit(solution)/shard_map/pallas_call | solution.py:647
  134.1 5.8 %shard_map.129 = (bf16[112,2048]{1,0:T(8,128)(2,1)}, bf16[112,2048]{1,0:T(8,128)(2,1)}, f32[256,1536]{1,0:T(8,128)}, f32[256,1536]{1,0:T(8,128)}, f32[1536,256]{1,0:T(8,128)}) custom-call(bf16[112,2048]{1,0:T(8,128)(2,1)} %get-tuple-element.10.refs_0_, bf16[112,2048]{1,0:T(8,128)(2,1)} %get-tuple-element.11.refs_1_, f32[256,1536]{1,0:T(8,128)} %refs_2_.1, ...), custom_call_target="tpu_custom_call" | custom-call | flops 1179648 | bytes 11796480 | tf_op jit(solution)/shard_map/pallas_call | solution.py:734
